TPU v7x, 1024 devices: a whole 4x8x16 slice. The times are simulated.
1024 devices in a mesh: ra: 128 (over z, y), cb: 8 (over x, core).
Axes of the slice: x: 4, y: 8, z: 16, core: 2. Of those that a mesh axis runs over, the one named last changes fastest.
Arguments:
- tokens: bfloat16 [512, 4096], P(None, 'cb'), may hold values from -400 to 400
- norm_gain: bfloat16 [4096], P('cb'), may hold values from 0.099609375 to 1.8984375
- w_gate: bfloat16 [4096, 11264], P('cb', 'ra'), may hold values from -0.09375 to 0.09375
- w_up: bfloat16 [4096, 11264], P('cb', 'ra'), may hold values from -0.09375 to 0.09375
- w_down: bfloat16 [11264, 4096], P('ra', 'cb'), may hold values from -0.0546875 to 0.0546875
- out_gain: bfloat16 [4096], P('cb'), may hold values from 0.099609375 to 1.8984375
Outputs:
- normed_out: bfloat16 [512, 4096], P('ra', 'cb')
All inputs are finite; a program needn't handle non-finite values.
Results may differ from a plain program's by a relative error of at most 0.0045.
Values sent between devices are 32-bit elements; how exact they have to be, the bound alone decides.
No kernel may reach another device: no remote copies, remote signals or barrier semaphores. Data moves between devices by JAX's collectives and lax.ppermute only.
A program may use at most 32 MiB of HBM per device.

v0:
```python
import jax
import jax.numpy as jnp
from jax import lax
from jax.sharding import Mesh
from jax.sharding import PartitionSpec as P

D = 4096
RA = ("ra_0", "ra_1")


def sent_to_all(array, axis):
    copies = jnp.broadcast_to(array, (lax.axis_size(axis), *array.shape))
    return lax.all_to_all(copies, axis, split_axis=0, concat_axis=0, tiled=True)


def over_copies(array, axis):
    return sent_to_all(array, axis).sum(axis=0)


def together(arrays, axis):
    ends = [0]
    for a in arrays:
        ends.append(ends[-1] + a.size)
    so_far = over_copies(jnp.concatenate([a.ravel() for a in arrays]), axis)
    return tuple((so_far[b:e].reshape(a.shape) for a, b, e in zip(arrays, ends, ends[1:])))


def summed_rows(array, axes, dim):
    for axis in axes:
        array = lax.psum_scatter(array, axis, scatter_dimension=dim, tiled=True)
    return array


def body(tokens, norm_gain, w_gate, w_up, w_down, out_gain):
    eps = 1e-06
    xfloat = tokens.astype(jnp.float32)
    local_sq = jnp.sum(xfloat * xfloat, axis=1)
    scaled = (xfloat * norm_gain.astype(jnp.float32)).astype(jnp.bfloat16)
    gate_part = jnp.dot(scaled, w_gate, preferred_element_type=jnp.float32)
    up_part = jnp.dot(scaled, w_up, preferred_element_type=jnp.float32)
    total_sq, gate_sum, up_sum = together((local_sq, gate_part, up_part), "cb")
    inv_in = lax.rsqrt(total_sq / D + eps)[:, None]
    hidden = (jax.nn.silu(gate_sum * inv_in) * (up_sum * inv_in)).astype(jnp.bfloat16)
    partial_down = jnp.dot(hidden, w_down, preferred_element_type=jnp.float32)
    own_rows = tokens.shape[0] // lax.axis_size(RA)
    first_row = lax.axis_index(RA) * own_rows
    down = summed_rows(partial_down, RA, 0)
    residual = lax.dynamic_slice_in_dim(xfloat, first_row, own_rows, 0)
    mixed = 0.1 * residual + down
    out_sq = over_copies(jnp.sum(mixed * mixed, axis=1), "cb")
    inv_out = lax.rsqrt(out_sq / D + eps)[:, None]
    return (mixed * inv_out * out_gain.astype(jnp.float32)).astype(jnp.bfloat16)


def solution(mesh):
    finer = Mesh(mesh.devices.reshape(16, 8, mesh.shape["cb"]), ("ra_0", "ra_1", "cb"))
    placed = (P(None, "cb"), P("cb"), P("cb", RA), P("cb", RA), P(RA, "cb"), P("cb"))
    return jax.shard_map(body, mesh=finer, in_specs=placed, out_specs=P(RA, "cb"), check_vma=False)
```

profile of v0, /device:TPU:1, one launch (start us, length us, event | category | flops | bytes accessed | tf_op | source)
XLA Modules:
  0.0 246.3 jit_solution(16246812147980231349)
XLA Ops:
  6.5 0.7 convert_element_type.19
  7.3 1.2 multiply_reduce_fusion
  8.5 1.3 fusion.1
  9.8 0.2 reshape.28
  10.0 1.3 fusion
  11.4 0.2 reshape.29
  11.6 1.5 broadcast_in_dim.4
  13.1 51.9 %all_to_all.12 = f32[8,1,90624]{2,1,0:T(1,128)S(1)} all-to-all(f32[8,1,90624]{2,1,0:T(1,128)S(1)} %broadcast_in_dim.4), channel_id=1, replica_groups=mesh['ra_0'=16,'ra_1'=8,'cb'=8] {'cb'}, dimensions={0} | all-to-all | bytes 5799936 | tf_op jit(solution)/shard_map/all_to_all | solution.py:13
  65.0 2.1 reduce_sum.37
  67.2 0.2 reshape.30
  67.4 0.2 reshape.31
  67.7 1.4 fusion.2
  69.1 0.0 reduce-scatter.2.cloned.1.call-update
  69.1 0.0 all-reduce.3.cloned.1.call-start
  69.1 59.9 %reduce-scatter.2.cloned.1.call-done = f32[32,512]{1,0:T(8,128)} async-done(((f32[512,512]{1,0:T(8,128)}), f32[32,512]{1,0:T(8,128)}) %reduce-scatter.2.cloned.1.call-update) | async-done | bytes 65552 | tf_op jit(solution)/shard_map/reduce_scatter | solution.py:30
  129.0 0.0 all-reduce.3.cloned.1.call-update
  129.1 0.1 convert_element_type.18
  129.2 1.3 dynamic-slice
  131.1 91.4 %all-reduce.3.cloned.1.call-done = f32[32,512]{1,0:T(8,128)} async-done(((f32[32,512]{1,0:T(8,128)}), f32[32,512]{1,0:T(8,128)}) %all-reduce.3.cloned.1.call-update) | async-done | bytes 65552
  222.5 0.8 multiply_reduce_fusion.1
  223.4 0.6 broadcast_in_dim.5
  224.0 9.5 %all-to-all-start.1 = ((f32[8,1,4]{2,1,0:T(1,128)}), f32[8,1,4]{2,1,0:T(1,128)S(1)}, u32[]{:S(2)}, u32[]{:S(2)}) async-start(f32[8,1,4]{2,1,0:T(1,128)} %broadcast_in_dim.5), calls=%async_computation.2 | async-start | bytes 8192 | tf_op jit(solution)/shard_map/all_to_all | solution.py:13
  233.5 4.5 %all-to-all-done.1 = f32[8,1,4]{2,1,0:T(1,128)S(1)} async-done(((f32[8,1,4]{2,1,0:T(1,128)}), f32[8,1,4]{2,1,0:T(1,128)S(1)}, u32[]{:S(2)}, u32[]{:S(2)}) %all-to-all-start.1) | async-done | bytes 160 | tf_op jit(solution)/shard_map/all_to_all | solution.py:13
  238.1 1.4 multiply_convert_fusion.5
  (13 shorter events, 0.1 us)
Async XLA Ops:
  6.5 61.2 %copy-start = (bf16[88,512]{1,0:T(8,128)(2,1)S(1)}, bf16[88,512]{1,0:T(8,128)(2,1)}, u32[]{:S(2)}) copy-start(bf16[88,512]{1,0:T(8,128)(2,1)} %param.10) | copy-start | bytes 270340
  6.5 122.5 %reduce-scatter.2.cloned.1.call-start = ((), (), s32[]{:S(2)}) async-start(), calls=%async_computation.3 | async-start | bytes 1114112 | tf_op jit(solution)/shard_map/reduce_scatter | solution.py:30
  67.1 61.9 %copy-start.1 = (bf16[512,512]{1,0:T(8,128)(2,1)S(1)}, bf16[512,512]{1,0:T(8,128)(2,1)}, u32[]{:S(2)}) copy-start(bf16[512,512]{1,0:T(8,128)(2,1)} %param.6) | copy-start | bytes 1572868
  67.1 166.4 %copy-start.2 = (bf16[512]{0:T(512)(128)(2,1)S(1)}, bf16[512]{0:T(512)(128)(2,1)}, u32[]{:S(2)}) copy-start(bf16[512]{0:T(512)(128)(2,1)} %param.11) | copy-start | bytes 3076
  69.1 153.5 %all-reduce.3.cloned.1.call-start = ((), (), s32[]{:S(2)}) async-start(), calls=%async_computation.4 | async-start | bytes 131072
  224.0 14.1 %all-to-all-start.1 = ((f32[8,1,4]{2,1,0:T(1,128)}), f32[8,1,4]{2,1,0:T(1,128)S(1)}, u32[]{:S(2)}, u32[]{:S(2)}) async-start(f32[8,1,4]{2,1,0:T(1,128)} %broadcast_in_dim.5), calls=%async_computation.2 | async-start | bytes 8192 | tf_op jit(solution)/shard_map/all_to_all | solution.py:13
Sparse Core Ops, SparseCore 0:
  69.2 59.7 reduce-scatter.1
  131.3 91.1 all-reduce.2
where the time goes:
time: 247 us; the launch traced here: 246 us
  waiting for transfers between devices  156 us (63%)
  blocking collectives  51.9 us (21%)
  between operations  14.2 us (6%)
  starting transfers between devices  9.58 us (4%)
  other arithmetic  6.45 us (3%)
  local copies, waits for them, and re-layouts  4.3 us (2%)
  matrix products  4.04 us (2%)
    unnamed x3, waiting for transfers between devices  91.4 us
    reduce_scatter x1, waiting for transfers between devices, summed_rows(): array = lax.psum_scatter(array, axis, scatter_dimension=dim, tiled=True)  59.9 us
    all_to_all x1, blocking collectives, sent_to_all(): return lax.all_to_all(copies, axis, split_axis=0, concat_axis=0, tiled=True)  51.9 us
    all_to_all x1, starting transfers between devices, sent_to_all(): return lax.all_to_all(copies, axis, split_axis=0, concat_axis=0, tiled=True)  9.54 us
  transfers between devices with their start and end apart: 3, of which 3 were waited for; matrix products, arithmetic and copies ran while one was open for 1% of the time, Pallas kernels for 0%

commit v1 on v0

v1 whole, which is shorter than its diff:
```python
import jax
import jax.numpy as jnp
from jax import lax
from jax.experimental import pallas as pl
from jax.experimental.pallas import tpu as pltpu
from jax.sharding import Mesh
from jax.sharding import PartitionSpec as P

D = 4096
EPS = 1e-06
RA = ("zq", "z0", "yq", "y0")
QUAD = ("z0", "y0")
REST = ("zq", "yq")
NT = (((1,), (1,)), ((), ()))
F32 = jnp.float32
BF16 = jnp.bfloat16
SMALL = pltpu.CompilerParams(vmem_limit_bytes=8 * 1024 * 1024)


def exchange(array, axes):
    return lax.all_to_all(array, axes, split_axis=0, concat_axis=0, tiled=True)


def front(tok, gain, wg, wu, out):
    x = tok[...].astype(F32)
    sq = jnp.sum(x * x, axis=1, keepdims=True)
    scaled = (x * gain[...].astype(F32)).astype(BF16)
    g = lax.dot_general(scaled, wg[...], NT, preferred_element_type=F32)
    u = lax.dot_general(scaled, wu[...], NT, preferred_element_type=F32)
    rows, units = g.shape
    fill = jnp.broadcast_to(sq, (rows, 128 - units))
    out[...] = jnp.concatenate([g, fill, u, fill], axis=1)


def middle(parts, out):
    n_z0, n_y0, n_cb, held, units = out.shape
    total = jnp.sum(parts[...], axis=0)
    inv = lax.rsqrt(total[:, units : units + 1] / D + EPS)
    g = total[:, :units] * inv
    u = total[:, 128 : 128 + units] * inv
    hidden = (g / (1.0 + jnp.exp(-g)) * u).astype(BF16).astype(F32)
    r = 4
    n_yq = held // r
    for a in range(n_z0):
        for b in range(n_y0):
            rows = [((a * n_yq + q) * n_y0 + b) * r for q in range(n_yq)]
            block = jnp.concatenate([hidden[s : s + r] for s in rows], axis=0)
            for j in range(n_cb):
                out[a, b, j] = block


def back(me, hid, w0, w1, w2, w3, out):
    acc = None
    for k, w in enumerate((w0, w1, w2, w3)):
        left = hid[me[0] ^ k].astype(BF16)
        part = jnp.dot(left, w[...].astype(BF16), preferred_element_type=F32)
        acc = part if acc is None else acc + part
    n, per, _ = out.shape
    for k in range(n):
        out[k] = acc[k * per : (k + 1) * per]


def fold(row, sums, tok, mixed, sq):
    n, per, _ = sums.shape
    down = jnp.sum(sums[...], axis=0)
    pair = tok[...].astype(F32)
    residual = jnp.where(row[0] % 2 == 1, pair[per:], pair[:per])
    value = 0.1 * residual + down
    mixed[...] = value
    total = jnp.sum(value * value, axis=1, keepdims=True)
    sq[...] = jnp.broadcast_to(total[None], sq.shape)


def finish(mixed, sq, gain, out):
    total = jnp.sum(sq[...], axis=0)[:, :1]
    inv = lax.rsqrt(total / D + EPS)
    out[...] = (mixed[...] * inv * gain[...].astype(F32)).astype(BF16)


def body(tokens, norm_gain, w_gate, w_up, w_down, out_gain):
    n_cb = lax.axis_size("cb")
    n_quad = lax.axis_size(QUAD)
    n_rest = lax.axis_size(REST)
    rows, cols = tokens.shape
    units = w_gate.shape[1]
    own = rows // lax.axis_size(RA)
    share = rows // n_cb
    held = share // n_quad

    mine = w_down.astype(F32)
    others = []
    for k in range(1, n_quad):
        with jax.named_scope(f"weights{k}"):
            others.append(lax.ppermute(mine, QUAD, [(i, i ^ k) for i in range(n_quad)]))

    partial = pl.pallas_call(front, out_shape=jax.ShapeDtypeStruct((rows, 256), F32), name="front", compiler_params=SMALL)(
        tokens, norm_gain[None, :], w_gate.T, w_up.T)
    with jax.named_scope("parts"):
        parts = exchange(partial.reshape(n_cb, share, 256), "cb")
    with jax.named_scope("gating"):
        blocks = pl.pallas_call(middle, out_shape=jax.ShapeDtypeStruct((2, 2, n_cb, held, units), F32), name="middle", compiler_params=SMALL)(parts)
    with jax.named_scope("spread"):
        got = exchange(blocks.reshape(n_quad * n_cb, held, units), QUAD + ("cb",))

    me = lax.axis_index(QUAD).astype(jnp.int32)[None]
    sums = pl.pallas_call(
        back,
        grid_spec=pltpu.PrefetchScalarGridSpec(num_scalar_prefetch=1, grid=(1,), in_specs=[
            pl.BlockSpec((n_quad, n_cb * held, units), lambda i, m: (0, 0, 0)),
            *[pl.BlockSpec((units, cols), lambda i, m: (0, 0))] * 4,
        ], out_specs=pl.BlockSpec((n_rest, own, cols), lambda i, m: (0, 0, 0))),
        out_shape=jax.ShapeDtypeStruct((n_rest, own, cols), F32), name="back", compiler_params=SMALL)(
        me, got.reshape(n_quad, n_cb * held, units), w_down, *others)
    with jax.named_scope("scatter"):
        sums = exchange(sums, REST)

    row = lax.axis_index(RA).astype(jnp.int32)[None]
    mixed, sq = pl.pallas_call(
        fold,
        grid_spec=pltpu.PrefetchScalarGridSpec(num_scalar_prefetch=1, grid=(1,), in_specs=[
            pl.BlockSpec((n_rest, own, cols), lambda i, m: (0, 0, 0)),
            pl.BlockSpec((2 * own, cols), lambda i, m: (m[0] // 2, 0)),
        ], out_specs=[pl.BlockSpec((own, cols), lambda i, m: (0, 0)), pl.BlockSpec((n_cb, own, 128), lambda i, m: (0, 0, 0))]),
        out_shape=[jax.ShapeDtypeStruct((own, cols), F32), jax.ShapeDtypeStruct((n_cb, own, 128), F32)], name="fold", compiler_params=SMALL)(
        row, sums, tokens)
    with jax.named_scope("norm"):
        sq = exchange(sq, "cb")
    return pl.pallas_call(finish, out_shape=jax.ShapeDtypeStruct((own, cols), BF16), name="finish", compiler_params=SMALL)(
        mixed, sq, out_gain[None, :])


def solution(mesh):
    finer = Mesh(mesh.devices.reshape(8, 2, 4, 2, mesh.shape["cb"]), (*RA, "cb"))
    placed = (P(None, "cb"), P("cb"), P("cb", RA), P("cb", RA), P(RA, "cb"), P("cb"))
    return jax.shard_map(body, mesh=finer, in_specs=placed, out_specs=P(RA, "cb"), check_vma=False)
```

time: 247 us -> 98.9 us (0.40)
  waiting for transfers between devices: 156 us -> 29.7 us
  blocking collectives: 51.9 us -> 25.8 us
  starting transfers between devices: 9.58 us -> 35.5 us
  between operations: 14.2 us -> 0.1 us
  other arithmetic: 6.45 us -> 0.01 us
  matrix products: 4.04 us -> 0 us
  Pallas kernels: 0 us -> 3.67 us
    unnamed x3 -> x0, waiting for transfers between devices: 91.4 us -> none
    reduce_scatter x1 -> x0, waiting for transfers between devices: 59.9 us -> none  [summed_rows(): array = lax.psum_scatter(array, axis, scatter_dimension=dim, tiled=True)]
    all_to_all x1, blocking collectives: 51.9 us -> 25.8 us  [exchange(): return lax.all_to_all(array, axes, split_axis=0, concat_axis=0, tiled=True)]
    all_to_all x1 -> x3, waiting for transfers between devices: 4.52 us -> 23.6 us  [exchange(): return lax.all_to_all(array, axes, split_axis=0, concat_axis=0, tiled=True)]
    all_to_all x1 -> x3, starting transfers between devices: 9.54 us -> 27.1 us  [exchange(): return lax.all_to_all(array, axes, split_axis=0, concat_axis=0, tiled=True)]
    ppermute x0 -> x3, starting transfers between devices: none -> 8.44 us  [body(): others.append(lax.ppermute(mine, QUAD, [(i, i ^ k) for i in range(n_quad)]))]
    ppermute x0 -> x3, waiting for transfers between devices: none -> 6.01 us  [body(): others.append(lax.ppermute(mine, QUAD, [(i, i ^ k) for i in range(n_quad)]))]
    reduce_sum x4 -> x0, other arithmetic: 4.19 us -> none  [the longest x2 2.13 us: over_copies(): return sent_to_all(array, axis).sum(axis=0)]
  transfers between devices with their start and end apart: 3 -> 6, of which waited for: 3 -> 5; matrix products, arithmetic and copies ran while one was open for 1% -> 0% of each run, Pallas kernels for 0% -> 0%
where the time goes in v1:
time: 98.9 us; the launch traced here: 98.3 us
  starting transfers between devices  35.5 us (36%)
  waiting for transfers between devices  29.7 us (30%)
  blocking collectives  25.8 us (26%)
  Pallas kernels  3.67 us (4%)
  local copies, waits for them, and re-layouts  3.52 us (4%)
    all_to_all x3, starting transfers between devices, exchange(): return lax.all_to_all(array, axes, split_axis=0, concat_axis=0, tiled=True)  27.1 us
    all_to_all x1, blocking collectives, exchange(): return lax.all_to_all(array, axes, split_axis=0, concat_axis=0, tiled=True)  25.8 us
    all_to_all x3, waiting for transfers between devices, exchange(): return lax.all_to_all(array, axes, split_axis=0, concat_axis=0, tiled=True)  23.6 us
    ppermute x3, starting transfers between devices, body(): others.append(lax.ppermute(mine, QUAD, [(i, i ^ k) for i in range(n_quad)]))  8.44 us
    ppermute x3, waiting for transfers between devices, body(): others.append(lax.ppermute(mine, QUAD, [(i, i ^ k) for i in range(n_quad)]))  6.01 us
    unnamed x12, local copies, waits for them, and re-layouts  2.83 us
  transfers between devices with their start and end apart: 6, of which 5 were waited for; matrix products, arithmetic and copies ran while one was open for 0% of the time, Pallas kernels for 0%

profile of v1, /device:TPU:1, one launch (start us, length us, event | category | flops | bytes accessed | tf_op | source)
XLA Modules:
  0.0 98.3 jit_solution(7586147523052149117)
XLA Ops:
  0.0 0.7 broadcast_in_dim.14.gain
  0.7 1.0 %copy-done = bf16[512,512]{1,0:T(8,128)(2,1)S(1)} copy-done((bf16[512,512]{1,0:T(8,128)(2,1)S(1)}, bf16[512,512]{1,0:T(8,128)(2,1)}, u32[]{:S(2)}) %copy-start) | copy-done | bytes 524312
  1.7 0.9 copy-done.3
  2.6 0.9 copy-done.4
  3.5 0.4 front.1
  3.9 25.8 %all_to_all.20.parts = f32[8,64,256]{2,1,0:T(8,128)S(1)} all-to-all(f32[8,64,256]{2,1,0:T(8,128)S(1)} %bitcast.7), channel_id=1, replica_groups=mesh['zq'=8,'z0'=2,'yq'=4,'y0'=2,'cb'=8] {'cb'}, dimensions={0} | all-to-all | bytes 1048576 | tf_op jit(solution)/shard_map/parts/all_to_all | solution.py:21
  29.8 0.8 middle.1
  30.6 4.7 %all-to-all-start.1 = ((f32[32,16,88]{2,1,0:T(8,128)}), f32[32,16,88]{2,1,0:T(8,128)S(1)}, u32[]{:S(2)}, u32[]{:S(2)}) async-start(f32[32,16,88]{2,1,0:T(8,128)} %bitcast.5), calls=%async_computation.1 | async-start | bytes 524288 | tf_op jit(solution)/shard_map/spread/all_to_all | solution.py:21
  35.3 0.0 copy-done.2
  35.3 3.3 %collective-permute-start = (f32[88,512]{1,0:T(8,128)S(1)}, f32[88,512]{1,0:T(8,128)S(1)}, u32[]{:S(2)}, u32[]{:S(2)}) collective-permute-start(f32[88,512]{1,0:T(8,128)S(1)} %convert_element_type.3), channel_id=1, source_target_pairs={{0,8},{8,0},{64,72},{72,64},{1,9},{9,1},{65,73},{73,65},{2,10},{10... | collective-permute-start | bytes 540680 | tf_op jit(solution)/shard_map/weights1/ppermute | solution.py:94
  38.7 3.2 %collective-permute-start.1 = (f32[88,512]{1,0:T(8,128)S(1)}, f32[88,512]{1,0:T(8,128)S(1)}, u32[]{:S(2)}, u32[]{:S(2)}) collective-permute-start(f32[88,512]{1,0:T(8,128)S(1)} %convert_element_type.3), channel_id=1, source_target_pairs={{0,64},{8,72},{64,0},{72,8},{1,65},{9,73},{65,1},{73,9},{2,66},{10... | collective-permute-start | bytes 540680 | tf_op jit(solution)/shard_map/weights2/ppermute | solution.py:94
  41.9 1.9 %collective-permute-start.2 = (f32[88,512]{1,0:T(8,128)S(1)}, f32[88,512]{1,0:T(8,128)S(1)}, u32[]{:S(2)}, u32[]{:S(2)}) collective-permute-start(f32[88,512]{1,0:T(8,128)S(1)} %convert_element_type.3), channel_id=1, source_target_pairs={{0,72},{8,64},{64,8},{72,0},{1,73},{9,65},{65,9},{73,1},{2,74},{10... | collective-permute-start | bytes 540680 | tf_op jit(solution)/shard_map/weights3/ppermute | solution.py:94
  43.8 0.5 collective-permute-done.w1
  44.3 1.7 %collective-permute-done.1.w2 = f32[88,512]{1,0:T(8,128)S(1)} collective-permute-done((f32[88,512]{1,0:T(8,128)S(1)}, f32[88,512]{1,0:T(8,128)S(1)}, u32[]{:S(2)}, u32[]{:S(2)}) %collective-permute-start.1) | collective-permute-done | bytes 180256 | tf_op jit(solution)/shard_map/weights2/ppermute | solution.py:94
  46.0 3.8 %collective-permute-done.2.w3 = f32[88,512]{1,0:T(8,128)S(1)} collective-permute-done((f32[88,512]{1,0:T(8,128)S(1)}, f32[88,512]{1,0:T(8,128)S(1)}, u32[]{:S(2)}, u32[]{:S(2)}) %collective-permute-start.2) | collective-permute-done | bytes 180256 | tf_op jit(solution)/shard_map/weights3/ppermute | solution.py:94
  49.8 0.0 all-to-all-done.1
  49.8 1.0 %back.1 = f32[32,4,512]{2,1,0:T(4,128)} custom-call(s32[1]{0:T(128)} %bitcast.1.me, f32[4,128,88]{2,1,0:T(8,128)S(1)} %bitcast.8, bf16[88,512]{1,0:T(8,128)(2,1)S(1)} %copy-done.2, f32[88,512]{1,0:T(8,128)S(1)} %collective-permute-done.w1, f32[88,512]{1,0:T(8,128)S(1)} %collective-permute-done.1.w2, f32[88,512]{1,0:T(8,128)S(1)} %collective-permute-done.2.w3), custom_call_target="tpu_custom_call" | custom-call | tf_op jit(solution)/shard_map/back/pallas_call | solution.py:106
  50.8 13.3 %all-to-all-start.2 = ((f32[32,4,512]{2,1,0:T(4,128)}), f32[32,4,512]{2,1,0:T(4,128)S(1)}, u32[]{:S(2)}, u32[]{:S(2)}) async-start(f32[32,4,512]{2,1,0:T(4,128)} %back.1), calls=%async_computation.2 | async-start | bytes 524288 | tf_op jit(solution)/shard_map/scatter/all_to_all | solution.py:21
  64.2 19.0 %all-to-all-done.2.sums = f32[32,4,512]{2,1,0:T(4,128)S(1)} async-done(((f32[32,4,512]{2,1,0:T(4,128)}), f32[32,4,512]{2,1,0:T(4,128)S(1)}, u32[]{:S(2)}, u32[]{:S(2)}) %all-to-all-start.2) | async-done | bytes 262176 | tf_op jit(solution)/shard_map/scatter/all_to_all | solution.py:21
  83.2 0.0 copy-done.1
  83.2 0.7 fold.1
  83.9 9.1 %all-to-all-start.3 = ((f32[8,4,128]{2,1,0:T(4,128)}), f32[8,4,128]{2,1,0:T(4,128)S(1)}, u32[]{:S(2)}, u32[]{:S(2)}) async-start(f32[8,4,128]{2,1,0:T(4,128)} %get-tuple-element.8), calls=%async_computation.3 | async-start | bytes 32768 | tf_op jit(solution)/shard_map/norm/all_to_all | solution.py:21
  93.0 4.6 %all-to-all-done.3.sq = f32[8,4,128]{2,1,0:T(4,128)S(1)} async-done(((f32[8,4,128]{2,1,0:T(4,128)}), f32[8,4,128]{2,1,0:T(4,128)S(1)}, u32[]{:S(2)}, u32[]{:S(2)}) %all-to-all-start.3) | async-done | bytes 16416 | tf_op jit(solution)/shard_map/norm/all_to_all | solution.py:21
  97.6 0.7 finish.1
  (9 shorter events, 0.0 us)
Async XLA Ops:
  0.7 1.0 %copy-start = (bf16[512,512]{1,0:T(8,128)(2,1)S(1)}, bf16[512,512]{1,0:T(8,128)(2,1)}, u32[]{:S(2)}) copy-start(bf16[512,512]{1,0:T(8,128)(2,1)} %tok.3) | copy-start | bytes 1572868
  1.7 0.9 copy-start.3
  2.6 0.9 copy-start.4
  30.6 4.7 %copy-start.2 = (bf16[88,512]{1,0:T(8,128)(2,1)S(1)}, bf16[88,512]{1,0:T(8,128)(2,1)}, u32[]{:S(2)}) copy-start(bf16[88,512]{1,0:T(8,128)(2,1)} %w0.1) | copy-start | bytes 270340
  30.6 19.2 %all-to-all-start.1 = ((f32[32,16,88]{2,1,0:T(8,128)}), f32[32,16,88]{2,1,0:T(8,128)S(1)}, u32[]{:S(2)}, u32[]{:S(2)}) async-start(f32[32,16,88]{2,1,0:T(8,128)} %bitcast.5), calls=%async_computation.1 | async-start | bytes 524288 | tf_op jit(solution)/shard_map/spread/all_to_all | solution.py:21
  35.3 9.0 %collective-permute-start = (f32[88,512]{1,0:T(8,128)S(1)}, f32[88,512]{1,0:T(8,128)S(1)}, u32[]{:S(2)}, u32[]{:S(2)}) collective-permute-start(f32[88,512]{1,0:T(8,128)S(1)} %convert_element_type.3), channel_id=1, source_target_pairs={{0,8},{8,0},{64,72},{72,64},{1,9},{9,1},{65,73},{73,65},{2,10},{10... | collective-permute-start | bytes 540680 | tf_op jit(solution)/shard_map/weights1/ppermute | solution.py:94
  38.7 7.3 %collective-permute-start.1 = (f32[88,512]{1,0:T(8,128)S(1)}, f32[88,512]{1,0:T(8,128)S(1)}, u32[]{:S(2)}, u32[]{:S(2)}) collective-permute-start(f32[88,512]{1,0:T(8,128)S(1)} %convert_element_type.3), channel_id=1, source_target_pairs={{0,64},{8,72},{64,0},{72,8},{1,65},{9,73},{65,1},{73,9},{2,66},{10... | collective-permute-start | bytes 540680 | tf_op jit(solution)/shard_map/weights2/ppermute | solution.py:94
  41.9 8.0 %collective-permute-start.2 = (f32[88,512]{1,0:T(8,128)S(1)}, f32[88,512]{1,0:T(8,128)S(1)}, u32[]{:S(2)}, u32[]{:S(2)}) collective-permute-start(f32[88,512]{1,0:T(8,128)S(1)} %convert_element_type.3), channel_id=1, source_target_pairs={{0,72},{8,64},{64,8},{72,0},{1,73},{9,65},{65,9},{73,1},{2,74},{10... | collective-permute-start | bytes 540680 | tf_op jit(solution)/shard_map/weights3/ppermute | solution.py:94
  50.8 32.3 %copy-start.1 = (bf16[512,512]{1,0:T(8,128)(2,1)S(1)}, bf16[512,512]{1,0:T(8,128)(2,1)}, u32[]{:S(2)}) copy-start(bf16[512,512]{1,0:T(8,128)(2,1)} %tok.3) | copy-start | bytes 1572868
  50.8 32.3 %all-to-all-start.2 = ((f32[32,4,512]{2,1,0:T(4,128)}), f32[32,4,512]{2,1,0:T(4,128)S(1)}, u32[]{:S(2)}, u32[]{:S(2)}) async-start(f32[32,4,512]{2,1,0:T(4,128)} %back.1), calls=%async_computation.2 | async-start | bytes 524288 | tf_op jit(solution)/shard_map/scatter/all_to_all | solution.py:21
  83.9 9.1 %copy-start.5 = (bf16[512]{0:T(512)(128)(2,1)S(1)}, bf16[512]{0:T(512)(128)(2,1)}, u32[]{:S(2)}) copy-start(bf16[512]{0:T(512)(128)(2,1)} %param.11) | copy-start | bytes 3076
  83.9 13.7 %all-to-all-start.3 = ((f32[8,4,128]{2,1,0:T(4,128)}), f32[8,4,128]{2,1,0:T(4,128)S(1)}, u32[]{:S(2)}, u32[]{:S(2)}) async-start(f32[8,4,128]{2,1,0:T(4,128)} %get-tuple-element.8), calls=%async_computation.3 | async-start | bytes 32768 | tf_op jit(solution)/shard_map/norm/all_to_all | solution.py:21

commit v2 on v1

v2 whole, which is shorter than its diff:
```python
import jax
import jax.numpy as jnp
from jax import lax
from jax.experimental import pallas as pl
from jax.experimental.pallas import tpu as pltpu
from jax.sharding import Mesh
from jax.sharding import PartitionSpec as P


D = 4096
EPS = 1e-06
RA = ("zq", "z0", "yq", "y0")
QUAD = ("z0", "y0")
REST = ("zq", "yq")
NT = (((1,), (1,)), ((), ()))
F32 = jnp.float32
BF16 = jnp.bfloat16
SMALL = pltpu.CompilerParams(vmem_limit_bytes=8 * 1024 * 1024)


def exchange(array, axes):
    return lax.all_to_all(array, axes, split_axis=0, concat_axis=0, tiled=True)


def copies(sources, targets, sems):
    started = [pltpu.make_async_copy(s, t, sems.at[k]) for k, (s, t) in enumerate(zip(sources, targets))]
    for c in started:
        c.start()
    return started


def front(tok_hbm, gain_hbm, wg_hbm, wu_hbm, out, tok, gain, wg, wu, sems):
    pending = copies((tok_hbm, gain_hbm, wg_hbm, wu_hbm), (tok, gain, wg, wu), sems)
    n_cb, _, lanes = out.shape
    rows, cols = tok.shape
    units = wg.shape[0]
    share = rows // n_cb
    half = share // 2
    first = lanes - units
    pending[0].wait()
    pending[1].wait()
    x = tok[...].astype(F32)
    sq = jnp.sum(x * x, axis=1, keepdims=True)
    scaled = (x * gain[...].astype(F32).reshape(1, cols)).astype(BF16)
    pending[2].wait()
    pending[3].wait()
    up = wu[...].astype(F32)
    left = jnp.concatenate([wg[...].astype(F32), up[:first]], axis=0).astype(BF16)
    gap = jnp.zeros((lanes // 2 - (units - first), cols), F32)
    none = jnp.zeros((lanes // 2, cols), F32)
    low = jnp.concatenate([up[first:], gap, none], axis=0).astype(BF16)
    high = jnp.concatenate([none, up[first:], gap], axis=0).astype(BF16)
    main = lax.dot_general(scaled, left, NT, preferred_element_type=F32)
    blocks = scaled.reshape(n_cb, 2, half, cols)
    sums = sq.reshape(n_cb, 2, half, 1)
    lane = lax.broadcasted_iota(jnp.int32, (n_cb * half, lanes), 1)
    rest = lax.dot_general(blocks[:, 0].reshape(n_cb * half, cols), low, NT, preferred_element_type=F32)
    rest = rest + lax.dot_general(blocks[:, 1].reshape(n_cb * half, cols), high, NT, preferred_element_type=F32)
    rest = jnp.where(lane == units - first, sums[:, 0].reshape(n_cb * half, 1), rest)
    rest = jnp.where(lane == lanes // 2 + units - first, sums[:, 1].reshape(n_cb * half, 1), rest)
    for j in range(n_cb):
        out[j, :share] = main[j * share : (j + 1) * share]
        out[j, share:] = rest[j * half : (j + 1) * half]


def middle(parts, out):
    n_z0, n_y0, n_cb, held, units = out.shape
    lanes = parts.shape[2]
    share = held * n_z0 * n_y0
    first = lanes - units
    total = parts[0]
    for k in range(1, n_cb):
        total = total + parts[k]
    main, rest = total[:share], total[share:]
    rest = jnp.concatenate([rest[:, : lanes // 2], rest[:, lanes // 2 :]], axis=0)
    inv = lax.rsqrt(rest[:, units - first : units - first + 1] / D + EPS)
    g = main[:, :units] * inv
    u = jnp.concatenate([main[:, units:], rest[:, : units - first]], axis=1) * inv
    hidden = (g / (1.0 + jnp.exp(-g)) * u).astype(BF16).astype(F32)
    r = 4
    n_yq = held // r
    for a in range(n_z0):
        for b in range(n_y0):
            rows = [((a * n_yq + q) * n_y0 + b) * r for q in range(n_yq)]
            block = jnp.concatenate([hidden[s : s + r] for s in rows], axis=0)
            for j in range(n_cb):
                out[a, b, j] = block


def back(here, hid, w0, w1, w2, w3, out):
    acc = None
    for k, w in enumerate((w0, w1, w2, w3)):
        left = hid[here[0] ^ k].astype(BF16)
        part = jnp.dot(left, w[...].astype(BF16), preferred_element_type=F32)
        acc = part if acc is None else acc + part
    n, per, _ = out.shape
    for k in range(n):
        out[k] = acc[k * per : (k + 1) * per]


def fold(here, sums, tok, mixed, sq):
    _, per, _ = sums.shape
    down = jnp.sum(sums[...], axis=0)
    pair = tok[...].astype(F32)
    residual = jnp.where(here[1] % 2 == 1, pair[per:], pair[:per])
    value = 0.1 * residual + down
    mixed[...] = value
    total = jnp.sum(value * value, axis=1, keepdims=True)
    sq[...] = jnp.broadcast_to(total[None], sq.shape)


def finish(mixed, sq, gain, out):
    total = jnp.sum(sq[...], axis=0)[:, :1]
    inv = lax.rsqrt(total / D + EPS)
    out[...] = (mixed[...] * inv * gain[...].astype(F32)).astype(BF16)


def body(tokens, norm_gain, w_gate, w_up, w_down, out_gain):
    n_cb = lax.axis_size("cb")
    n_quad = lax.axis_size(QUAD)
    n_rest = lax.axis_size(REST)
    rows, cols = tokens.shape
    units = w_gate.shape[1]
    own = rows // lax.axis_size(RA)
    share = rows // n_cb
    held = share // n_quad

    mine = w_down.astype(F32)
    others = []
    for k in range(1, n_quad):
        others.append(lax.ppermute(mine, QUAD, [(i, i ^ k) for i in range(n_quad)]))

    lanes = 128
    packed = share + share // 2
    partial = pl.pallas_call(
        front, in_specs=[pl.BlockSpec(memory_space=pltpu.HBM)] * 4,
        out_shape=jax.ShapeDtypeStruct((n_cb, packed, lanes), F32),
        scratch_shapes=[pltpu.VMEM((rows, cols), BF16), pltpu.VMEM((cols,), BF16), pltpu.VMEM((units, cols), BF16),
                        pltpu.VMEM((units, cols), BF16), pltpu.SemaphoreType.DMA((4,))],
        name="front")(tokens, norm_gain, w_gate.T, w_up.T)
    parts = exchange(partial, "cb")
    blocks = pl.pallas_call(middle, out_shape=jax.ShapeDtypeStruct((2, 2, n_cb, held, units), F32), name="middle", compiler_params=SMALL)(parts)
    got = exchange(blocks.reshape(n_quad * n_cb, held, units), QUAD + ("cb",))

    here = jnp.stack([lax.axis_index(QUAD), lax.axis_index(RA)]).astype(jnp.int32)
    sums = pl.pallas_call(
        back,
        grid_spec=pltpu.PrefetchScalarGridSpec(num_scalar_prefetch=1, grid=(1,), in_specs=[
            pl.BlockSpec((n_quad, n_cb * held, units), lambda i, m: (0, 0, 0)),
            *[pl.BlockSpec((units, cols), lambda i, m: (0, 0))] * 4,
        ], out_specs=pl.BlockSpec((n_rest, own, cols), lambda i, m: (0, 0, 0))),
        out_shape=jax.ShapeDtypeStruct((n_rest, own, cols), F32), name="back", compiler_params=SMALL)(
        here, got.reshape(n_quad, n_cb * held, units), w_down, *others)
    sums = exchange(sums, REST)

    mixed, sq = pl.pallas_call(
        fold,
        grid_spec=pltpu.PrefetchScalarGridSpec(num_scalar_prefetch=1, grid=(1,), in_specs=[
            pl.BlockSpec((n_rest, own, cols), lambda i, m: (0, 0, 0)),
            pl.BlockSpec((2 * own, cols), lambda i, m: (m[1] // 2, 0)),
        ], out_specs=[pl.BlockSpec((own, cols), lambda i, m: (0, 0)), pl.BlockSpec((n_cb, own, 128), lambda i, m: (0, 0, 0))]),
        out_shape=[jax.ShapeDtypeStruct((own, cols), F32), jax.ShapeDtypeStruct((n_cb, own, 128), F32)], name="fold", compiler_params=SMALL)(
        here, sums, tokens)
    sq = exchange(sq, "cb")
    return pl.pallas_call(finish, out_shape=jax.ShapeDtypeStruct((own, cols), BF16), name="finish", compiler_params=SMALL)(
        mixed, sq, out_gain[None, :])


def solution(mesh):
    finer = Mesh(mesh.devices.reshape(8, 2, 4, 2, mesh.shape["cb"]), (*RA, "cb"))
    placed = (P(None, "cb"), P("cb"), P("cb", RA), P("cb", RA), P(RA, "cb"), P("cb"))
    return jax.shard_map(body, mesh=finer, in_specs=placed, out_specs=P(RA, "cb"), check_vma=False)
```

time: 98.9 us -> 96.4 us (0.975)
  blocking collectives: 25.8 us -> 56.9 us
  waiting for transfers between devices: 29.7 us -> 10.6 us
  starting transfers between devices: 35.5 us -> 22 us
  local copies, waits for them, and re-layouts: 3.52 us -> 0.02 us
  Pallas kernels: 3.67 us -> 6.17 us
    all_to_all x1 -> x2, blocking collectives: 25.8 us -> 56.9 us  [exchange(): return lax.all_to_all(array, axes, split_axis=0, concat_axis=0, tiled=True)]
    all_to_all x3 -> x2, waiting for transfers between devices: 23.6 us -> 4.65 us  [exchange(): return lax.all_to_all(array, axes, split_axis=0, concat_axis=0, tiled=True)]
    all_to_all x3 -> x2, starting transfers between devices: 27.1 us -> 13.6 us  [exchange(): return lax.all_to_all(array, axes, split_axis=0, concat_axis=0, tiled=True)]
    unnamed x12 -> x6, local copies, waits for them, and re-layouts: 2.83 us -> 0.01 us
    pallas_call x1, Pallas kernels: 0.43 us -> 2.48 us  [body(): pl.pallas_call(front, in_specs=[pl.BlockSpec(memory_space=pltpu.HBM)] * 4...]
  transfers between devices with their start and end apart: 6 -> 5, of which waited for: 5 -> 4; matrix products, arithmetic and copies ran while one was open for 0% -> 0% of each run, Pallas kernels for 0% -> 0%
where the time goes in v2:
time: 96.4 us; the launch traced here: 95.9 us
  blocking collectives  56.9 us (59%)
  starting transfers between devices  22 us (23%)
  waiting for transfers between devices  10.6 us (11%)
  Pallas kernels  6.17 us (6%)
    all_to_all x2, blocking collectives, exchange(): return lax.all_to_all(array, axes, split_axis=0, concat_axis=0, tiled=True)  56.9 us
    all_to_all x2, starting transfers between devices, exchange(): return lax.all_to_all(array, axes, split_axis=0, concat_axis=0, tiled=True)  13.6 us
    ppermute x3, starting transfers between devices, body(): others.append(lax.ppermute(mine, QUAD, [(i, i ^ k) for i in range(n_quad)]))  8.44 us
    ppermute x3, waiting for transfers between devices, body(): others.append(lax.ppermute(mine, QUAD, [(i, i ^ k) for i in range(n_quad)]))  5.94 us
    all_to_all x2, waiting for transfers between devices, exchange(): return lax.all_to_all(array, axes, split_axis=0, concat_axis=0, tiled=True)  4.65 us
    pallas_call x1, Pallas kernels, body(): pl.pallas_call(front, in_specs=[pl.BlockSpec(memory_space=pltpu.HBM)] * 4...  2.48 us
  transfers between devices with their start and end apart: 5, of which 4 were waited for; matrix products, arithmetic and copies ran while one was open for 0% of the time, Pallas kernels for 0%

profile of v2, /device:TPU:1, one launch (start us, length us, event | category | flops | bytes accessed | tf_op | source)
XLA Modules:
  0.0 95.9 jit_solution(10645158925629754334)
XLA Ops:
  0.0 2.5 %front.1 = f32[8,96,128]{2,1,0:T(8,128)} custom-call(bf16[512,512]{1,0:T(8,128)(2,1)} %tok.1, bf16[512]{0:T(512)(128)(2,1)} %gain_hbm.1, bf16[88,512]{1,0:T(8,128)(2,1)} %bitcast.7, bf16[88,512]{1,0:T(8,128)(2,1)} %bitcast.8), custom_call_target="tpu_custom_call" | custom-call | tf_op jit(solution)/shard_map/front/pallas_call | solution.py:135
  2.5 25.5 %all_to_all.20.parts = f32[8,96,128]{2,1,0:T(8,128)S(1)} all-to-all(f32[8,96,128]{2,1,0:T(8,128)} %front.1), channel_id=1, replica_groups=mesh['zq'=8,'z0'=2,'yq'=4,'y0'=2,'cb'=8] {'cb'}, dimensions={0} | all-to-all | bytes 786432 | tf_op jit(solution)/shard_map/all_to_all | solution.py:22
  28.0 0.9 middle.1
  28.9 0.0 copy-start.1
  28.9 4.5 %all-to-all-start.1 = ((f32[32,16,88]{2,1,0:T(8,128)}), f32[32,16,88]{2,1,0:T(8,128)S(1)}, u32[]{:S(2)}, u32[]{:S(2)}) async-start(f32[32,16,88]{2,1,0:T(8,128)} %bitcast.4), calls=%async_computation.1 | async-start | bytes 524288 | tf_op jit(solution)/shard_map/all_to_all | solution.py:22
  33.4 0.0 copy-done.1
  33.5 3.3 %collective-permute-start = (f32[88,512]{1,0:T(8,128)S(1)}, f32[88,512]{1,0:T(8,128)S(1)}, u32[]{:S(2)}, u32[]{:S(2)}) collective-permute-start(f32[88,512]{1,0:T(8,128)S(1)} %convert_element_type.3), channel_id=1, source_target_pairs={{0,8},{8,0},{64,72},{72,64},{1,9},{9,1},{65,73},{73,65},{2,10},{10... | collective-permute-start | bytes 540680 | tf_op jit(solution)/shard_map/ppermute | solution.py:131
  36.8 3.2 %collective-permute-start.1 = (f32[88,512]{1,0:T(8,128)S(1)}, f32[88,512]{1,0:T(8,128)S(1)}, u32[]{:S(2)}, u32[]{:S(2)}) collective-permute-start(f32[88,512]{1,0:T(8,128)S(1)} %convert_element_type.3), channel_id=1, source_target_pairs={{0,64},{8,72},{64,0},{72,8},{1,65},{9,73},{65,1},{73,9},{2,66},{10... | collective-permute-start | bytes 540680 | tf_op jit(solution)/shard_map/ppermute | solution.py:131
  40.0 1.9 %collective-permute-start.2 = (f32[88,512]{1,0:T(8,128)S(1)}, f32[88,512]{1,0:T(8,128)S(1)}, u32[]{:S(2)}, u32[]{:S(2)}) collective-permute-start(f32[88,512]{1,0:T(8,128)S(1)} %convert_element_type.3), channel_id=1, source_target_pairs={{0,72},{8,64},{64,8},{72,0},{1,73},{9,65},{65,9},{73,1},{2,74},{10... | collective-permute-start | bytes 540680 | tf_op jit(solution)/shard_map/ppermute | solution.py:131
  41.9 0.1 pad_add_fusion.here
  42.0 0.4 collective-permute-done.w1
  42.5 1.7 %collective-permute-done.1.w2 = f32[88,512]{1,0:T(8,128)S(1)} collective-permute-done((f32[88,512]{1,0:T(8,128)S(1)}, f32[88,512]{1,0:T(8,128)S(1)}, u32[]{:S(2)}, u32[]{:S(2)}) %collective-permute-start.1) | collective-permute-done | bytes 180256 | tf_op jit(solution)/shard_map/ppermute | solution.py:131
  44.1 3.8 %collective-permute-done.2.w3 = f32[88,512]{1,0:T(8,128)S(1)} collective-permute-done((f32[88,512]{1,0:T(8,128)S(1)}, f32[88,512]{1,0:T(8,128)S(1)}, u32[]{:S(2)}, u32[]{:S(2)}) %collective-permute-start.2) | collective-permute-done | bytes 180256 | tf_op jit(solution)/shard_map/ppermute | solution.py:131
  48.0 0.0 all-to-all-done.1
  48.0 0.8 back.1
  48.8 0.0 copy-start
  48.8 31.4 %all_to_all.21.sums = f32[32,4,512]{2,1,0:T(4,128)S(1)} all-to-all(f32[32,4,512]{2,1,0:T(4,128)S(1)} %back.1), channel_id=1, replica_groups=mesh['zq'=8,'z0'=2,'yq'=4,'y0'=2,'cb'=8] {'zq','yq'}, dimensions={0} | all-to-all | bytes 524288 | tf_op jit(solution)/shard_map/all_to_all | solution.py:22
  80.2 0.0 copy-done
  80.2 1.3 %fold.1 = (f32[4,512]{1,0:T(4,128)S(1)}, f32[8,4,128]{2,1,0:T(4,128)}) custom-call(s32[2]{0:T(128)S(1)} %pad_add_fusion.here, f32[32,4,512]{2,1,0:T(4,128)S(1)} %all_to_all.21.sums, bf16[512,512]{1,0:T(8,128)(2,1)S(1)} %copy-done), custom_call_target="tpu_custom_call" | custom-call | tf_op jit(solution)/shard_map/fold/pallas_call | solution.py:156
  81.5 0.0 copy-start.2
  81.5 9.1 %all-to-all-start.3 = ((f32[8,4,128]{2,1,0:T(4,128)}), f32[8,4,128]{2,1,0:T(4,128)S(1)}, u32[]{:S(2)}, u32[]{:S(2)}) async-start(f32[8,4,128]{2,1,0:T(4,128)} %get-tuple-element.8), calls=%async_computation.3 | async-start | bytes 32768 | tf_op jit(solution)/shard_map/all_to_all | solution.py:22
  90.6 0.0 copy-done.2
  90.6 4.6 %all-to-all-done.3.sq = f32[8,4,128]{2,1,0:T(4,128)S(1)} async-done(((f32[8,4,128]{2,1,0:T(4,128)}), f32[8,4,128]{2,1,0:T(4,128)S(1)}, u32[]{:S(2)}, u32[]{:S(2)}) %all-to-all-start.3) | async-done | bytes 16416 | tf_op jit(solution)/shard_map/all_to_all | solution.py:22
  95.2 0.7 finish.1
  (2 shorter events, 0.0 us)
Async XLA Ops:
  28.9 4.5 %copy-start.1 = (bf16[88,512]{1,0:T(8,128)(2,1)S(1)}, bf16[88,512]{1,0:T(8,128)(2,1)}, u32[]{:S(2)}) copy-start(bf16[88,512]{1,0:T(8,128)(2,1)} %w0.1) | copy-start | bytes 270340
  28.9 19.0 %all-to-all-start.1 = ((f32[32,16,88]{2,1,0:T(8,128)}), f32[32,16,88]{2,1,0:T(8,128)S(1)}, u32[]{:S(2)}, u32[]{:S(2)}) async-start(f32[32,16,88]{2,1,0:T(8,128)} %bitcast.4), calls=%async_computation.1 | async-start | bytes 524288 | tf_op jit(solution)/shard_map/all_to_all | solution.py:22
  33.5 9.0 %collective-permute-start = (f32[88,512]{1,0:T(8,128)S(1)}, f32[88,512]{1,0:T(8,128)S(1)}, u32[]{:S(2)}, u32[]{:S(2)}) collective-permute-start(f32[88,512]{1,0:T(8,128)S(1)} %convert_element_type.3), channel_id=1, source_target_pairs={{0,8},{8,0},{64,72},{72,64},{1,9},{9,1},{65,73},{73,65},{2,10},{10... | collective-permute-start | bytes 540680 | tf_op jit(solution)/shard_map/ppermute | solution.py:131
  36.8 7.3 %collective-permute-start.1 = (f32[88,512]{1,0:T(8,128)S(1)}, f32[88,512]{1,0:T(8,128)S(1)}, u32[]{:S(2)}, u32[]{:S(2)}) collective-permute-start(f32[88,512]{1,0:T(8,128)S(1)} %convert_element_type.3), channel_id=1, source_target_pairs={{0,64},{8,72},{64,0},{72,8},{1,65},{9,73},{65,1},{73,9},{2,66},{10... | collective-permute-start | bytes 540680 | tf_op jit(solution)/shard_map/ppermute | solution.py:131
  40.0 8.0 %collective-permute-start.2 = (f32[88,512]{1,0:T(8,128)S(1)}, f32[88,512]{1,0:T(8,128)S(1)}, u32[]{:S(2)}, u32[]{:S(2)}) collective-permute-start(f32[88,512]{1,0:T(8,128)S(1)} %convert_element_type.3), channel_id=1, source_target_pairs={{0,72},{8,64},{64,8},{72,0},{1,73},{9,65},{65,9},{73,1},{2,74},{10... | collective-permute-start | bytes 540680 | tf_op jit(solution)/shard_map/ppermute | solution.py:131
  48.8 31.4 %copy-start = (bf16[512,512]{1,0:T(8,128)(2,1)S(1)}, bf16[512,512]{1,0:T(8,128)(2,1)}, u32[]{:S(2)}) copy-start(bf16[512,512]{1,0:T(8,128)(2,1)} %tok.1) | copy-start | bytes 1572868
  81.5 9.1 %copy-start.2 = (bf16[512]{0:T(512)(128)(2,1)S(1)}, bf16[512]{0:T(512)(128)(2,1)}, u32[]{:S(2)}) copy-start(bf16[512]{0:T(512)(128)(2,1)} %param.11) | copy-start | bytes 3076
  81.5 13.7 %all-to-all-start.3 = ((f32[8,4,128]{2,1,0:T(4,128)}), f32[8,4,128]{2,1,0:T(4,128)S(1)}, u32[]{:S(2)}, u32[]{:S(2)}) async-start(f32[8,4,128]{2,1,0:T(4,128)} %get-tuple-element.8), calls=%async_computation.3 | async-start | bytes 32768 | tf_op jit(solution)/shard_map/all_to_all | solution.py:22

commit v3 on v2

--- a/solution.py
+++ b/solution.py
@@ -30,37 +30,40 @@
 
 
 def front(tok_hbm, gain_hbm, wg_hbm, wu_hbm, out, tok, gain, wg, wu, sems):
-    pending = copies((tok_hbm, gain_hbm, wg_hbm, wu_hbm), (tok, gain, wg, wu), sems)
     n_cb, _, lanes = out.shape
-    rows, cols = tok.shape
+    n_chunk, chunk, cols = tok.shape
     units = wg.shape[0]
-    share = rows // n_cb
+    share = n_chunk * chunk // n_cb
     half = share // 2
     first = lanes - units
+    chunks = [tok_hbm.at[pl.ds(c * chunk, chunk)] for c in range(n_chunk)]
+    pending = copies((wg_hbm, wu_hbm, gain_hbm, *chunks), (wg, wu, gain, *[tok.at[c] for c in range(n_chunk)]), sems)
     pending[0].wait()
     pending[1].wait()
-    x = tok[...].astype(F32)
-    sq = jnp.sum(x * x, axis=1, keepdims=True)
-    scaled = (x * gain[...].astype(F32).reshape(1, cols)).astype(BF16)
-    pending[2].wait()
-    pending[3].wait()
     up = wu[...].astype(F32)
     left = jnp.concatenate([wg[...].astype(F32), up[:first]], axis=0).astype(BF16)
     gap = jnp.zeros((lanes // 2 - (units - first), cols), F32)
     none = jnp.zeros((lanes // 2, cols), F32)
     low = jnp.concatenate([up[first:], gap, none], axis=0).astype(BF16)
     high = jnp.concatenate([none, up[first:], gap], axis=0).astype(BF16)
-    main = lax.dot_general(scaled, left, NT, preferred_element_type=F32)
-    blocks = scaled.reshape(n_cb, 2, half, cols)
-    sums = sq.reshape(n_cb, 2, half, 1)
-    lane = lax.broadcasted_iota(jnp.int32, (n_cb * half, lanes), 1)
-    rest = lax.dot_general(blocks[:, 0].reshape(n_cb * half, cols), low, NT, preferred_element_type=F32)
-    rest = rest + lax.dot_general(blocks[:, 1].reshape(n_cb * half, cols), high, NT, preferred_element_type=F32)
-    rest = jnp.where(lane == units - first, sums[:, 0].reshape(n_cb * half, 1), rest)
-    rest = jnp.where(lane == lanes // 2 + units - first, sums[:, 1].reshape(n_cb * half, 1), rest)
-    for j in range(n_cb):
-        out[j, :share] = main[j * share : (j + 1) * share]
-        out[j, share:] = rest[j * half : (j + 1) * half]
+    pending[2].wait()
+    scale = gain[...].astype(F32).reshape(1, cols)
+    per = chunk // share
+    lane = lax.broadcasted_iota(jnp.int32, (per * half, lanes), 1)
+    for c in range(n_chunk):
+        pending[3 + c].wait()
+        x = tok[c].astype(F32)
+        sq = jnp.sum(x * x, axis=1, keepdims=True)
+        scaled = (x * scale).astype(BF16)
+        main = lax.dot_general(scaled, left, NT, preferred_element_type=F32)
+        cut = lambda v, h: jnp.concatenate([v[p * share + h * half : p * share + (h + 1) * half] for p in range(per)], axis=0)
+        rest = lax.dot_general(cut(scaled, 0), low, NT, preferred_element_type=F32)
+        rest = rest + lax.dot_general(cut(scaled, 1), high, NT, preferred_element_type=F32)
+        rest = jnp.where(lane == units - first, cut(sq, 0), rest)
+        rest = jnp.where(lane == lanes // 2 + units - first, cut(sq, 1), rest)
+        for p in range(per):
+            out[c * per + p, :share] = main[p * share : (p + 1) * share]
+            out[c * per + p, share:] = rest[p * half : (p + 1) * half]
 
 
 def middle(parts, out):
@@ -98,21 +101,16 @@
         out[k] = acc[k * per : (k + 1) * per]
 
 
-def fold(here, sums, tok, mixed, sq):
-    _, per, _ = sums.shape
-    down = jnp.sum(sums[...], axis=0)
-    pair = tok[...].astype(F32)
-    residual = jnp.where(here[1] % 2 == 1, pair[per:], pair[:per])
-    value = 0.1 * residual + down
-    mixed[...] = value
+def fold(sums, residual, gain, gained, sq):
+    value = 0.1 * residual[...].astype(F32) + jnp.sum(sums[...], axis=0)
+    gained[...] = value * gain[...].astype(F32)
     total = jnp.sum(value * value, axis=1, keepdims=True)
     sq[...] = jnp.broadcast_to(total[None], sq.shape)
 
 
-def finish(mixed, sq, gain, out):
+def finish(gained, sq, out):
     total = jnp.sum(sq[...], axis=0)[:, :1]
-    inv = lax.rsqrt(total / D + EPS)
-    out[...] = (mixed[...] * inv * gain[...].astype(F32)).astype(BF16)
+    out[...] = (gained[...] * lax.rsqrt(total / D + EPS)).astype(BF16)
 
 
 def body(tokens, norm_gain, w_gate, w_up, w_down, out_gain):
@@ -135,14 +133,14 @@
     partial = pl.pallas_call(
         front, in_specs=[pl.BlockSpec(memory_space=pltpu.HBM)] * 4,
         out_shape=jax.ShapeDtypeStruct((n_cb, packed, lanes), F32),
-        scratch_shapes=[pltpu.VMEM((rows, cols), BF16), pltpu.VMEM((cols,), BF16), pltpu.VMEM((units, cols), BF16),
-                        pltpu.VMEM((units, cols), BF16), pltpu.SemaphoreType.DMA((4,))],
+        scratch_shapes=[pltpu.VMEM((4, rows // 4, cols), BF16), pltpu.VMEM((cols,), BF16), pltpu.VMEM((units, cols), BF16),
+                        pltpu.VMEM((units, cols), BF16), pltpu.SemaphoreType.DMA((7,))],
         name="front")(tokens, norm_gain, w_gate.T, w_up.T)
     parts = exchange(partial, "cb")
     blocks = pl.pallas_call(middle, out_shape=jax.ShapeDtypeStruct((2, 2, n_cb, held, units), F32), name="middle", compiler_params=SMALL)(parts)
     got = exchange(blocks.reshape(n_quad * n_cb, held, units), QUAD + ("cb",))
 
-    here = jnp.stack([lax.axis_index(QUAD), lax.axis_index(RA)]).astype(jnp.int32)
+    here = lax.axis_index(QUAD).astype(jnp.int32)[None]
     sums = pl.pallas_call(
         back,
         grid_spec=pltpu.PrefetchScalarGridSpec(num_scalar_prefetch=1, grid=(1,), in_specs=[
@@ -153,17 +151,12 @@
         here, got.reshape(n_quad, n_cb * held, units), w_down, *others)
     sums = exchange(sums, REST)
 
-    mixed, sq = pl.pallas_call(
-        fold,
-        grid_spec=pltpu.PrefetchScalarGridSpec(num_scalar_prefetch=1, grid=(1,), in_specs=[
-            pl.BlockSpec((n_rest, own, cols), lambda i, m: (0, 0, 0)),
-            pl.BlockSpec((2 * own, cols), lambda i, m: (m[1] // 2, 0)),
-        ], out_specs=[pl.BlockSpec((own, cols), lambda i, m: (0, 0)), pl.BlockSpec((n_cb, own, 128), lambda i, m: (0, 0, 0))]),
-        out_shape=[jax.ShapeDtypeStruct((own, cols), F32), jax.ShapeDtypeStruct((n_cb, own, 128), F32)], name="fold", compiler_params=SMALL)(
-        here, sums, tokens)
+    residual = lax.dynamic_slice_in_dim(tokens, lax.axis_index(RA) * own, own, 0)
+    gained, sq = pl.pallas_call(
+        fold, out_shape=[jax.ShapeDtypeStruct((own, cols), F32), jax.ShapeDtypeStruct((n_cb, own, 128), F32)], name="fold", compiler_params=SMALL)(
+        sums, residual, out_gain[None, :])
     sq = exchange(sq, "cb")
-    return pl.pallas_call(finish, out_shape=jax.ShapeDtypeStruct((own, cols), BF16), name="finish", compiler_params=SMALL)(
-        mixed, sq, out_gain[None, :])
+    return pl.pallas_call(finish, out_shape=jax.ShapeDtypeStruct((own, cols), BF16), name="finish", compiler_params=SMALL)(gained, sq)
 
 
 def solution(mesh):

time: 96.4 us -> 95.6 us (level)
  blocking collectives: 56.9 us -> 38.9 us
  waiting for transfers between devices: 10.6 us -> 23.6 us
  starting transfers between devices: 22 us -> 25.4 us
  local copies, waits for them, and re-layouts: 0.02 us -> 1.38 us
    all_to_all x2, blocking collectives: 56.9 us -> 38.9 us  [exchange(): return lax.all_to_all(array, axes, split_axis=0, concat_axis=0, tiled=True)]
    all_to_all x2, waiting for transfers between devices: 4.65 us -> 17.6 us  [exchange(): return lax.all_to_all(array, axes, split_axis=0, concat_axis=0, tiled=True)]
    all_to_all x2, starting transfers between devices: 13.6 us -> 17 us  [exchange(): return lax.all_to_all(array, axes, split_axis=0, concat_axis=0, tiled=True)]
    pallas_call x1, Pallas kernels: 1.29 us -> 0.14 us  [body(): pl.pallas_call(fold, out_shape=[jax.ShapeDtypeStruct((own, cols), F32), j...]
  transfers between devices with their start and end apart: 5 -> 5, of which waited for: 4 -> 4; matrix products, arithmetic and copies ran while one was open for 0% -> 1% of each run, Pallas kernels for 0% -> 0%
where the time goes in v3:
time: 95.6 us; the launch traced here: 95 us
  blocking collectives  38.9 us (41%)
  starting transfers between devices  25.4 us (27%)
  waiting for transfers between devices  23.6 us (25%)
  Pallas kernels  5.56 us (6%)
  local copies, waits for them, and re-layouts  1.38 us (1%)
    all_to_all x2, blocking collectives, exchange(): return lax.all_to_all(array, axes, split_axis=0, concat_axis=0, tiled=True)  38.9 us
    all_to_all x2, waiting for transfers between devices, exchange(): return lax.all_to_all(array, axes, split_axis=0, concat_axis=0, tiled=True)  17.6 us
    all_to_all x2, starting transfers between devices, exchange(): return lax.all_to_all(array, axes, split_axis=0, concat_axis=0, tiled=True)  17 us
    ppermute x3, starting transfers between devices, body(): others.append(lax.ppermute(mine, QUAD, [(i, i ^ k) for i in range(n_quad)]))  8.44 us
    ppermute x3, waiting for transfers between devices, body(): others.append(lax.ppermute(mine, QUAD, [(i, i ^ k) for i in range(n_quad)]))  6.01 us
    pallas_call x1, Pallas kernels, body(): pl.pallas_call(front, in_specs=[pl.BlockSpec(memory_space=pltpu.HBM)] * 4...  2.86 us
  transfers between devices with their start and end apart: 5, of which 4 were waited for; matrix products, arithmetic and copies ran while one was open for 1% of the time, Pallas kernels for 0%

profile of v3, /device:TPU:1, one launch (start us, length us, event | category | flops | bytes accessed | tf_op | source)
XLA Modules:
  0.0 95.0 jit_solution(12623254262696602875)
XLA Ops:
  0.0 2.9 %front.1 = f32[8,96,128]{2,1,0:T(8,128)} custom-call(bf16[512,512]{1,0:T(8,128)(2,1)} %tok_hbm.1, bf16[512]{0:T(512)(128)(2,1)} %gain_hbm.1, bf16[88,512]{1,0:T(8,128)(2,1)} %bitcast.6, bf16[88,512]{1,0:T(8,128)(2,1)} %bitcast.7), custom_call_target="tpu_custom_call" | custom-call | tf_op jit(solution)/shard_map/front/pallas_call | solution.py:133
  2.9 25.5 %all_to_all.20.parts = f32[8,96,128]{2,1,0:T(8,128)S(1)} all-to-all(f32[8,96,128]{2,1,0:T(8,128)} %front.1), channel_id=1, replica_groups=mesh['zq'=8,'z0'=2,'yq'=4,'y0'=2,'cb'=8] {'cb'}, dimensions={0} | all-to-all | bytes 786432 | tf_op jit(solution)/shard_map/all_to_all | solution.py:22
  28.4 0.9 middle.1
  29.3 0.0 copy-start
  29.3 4.5 %all-to-all-start.1 = ((f32[32,16,88]{2,1,0:T(8,128)}), f32[32,16,88]{2,1,0:T(8,128)S(1)}, u32[]{:S(2)}, u32[]{:S(2)}) async-start(f32[32,16,88]{2,1,0:T(8,128)} %bitcast.3), calls=%async_computation.1 | async-start | bytes 524288 | tf_op jit(solution)/shard_map/all_to_all | solution.py:22
  33.8 0.0 copy-done
  33.8 3.3 %collective-permute-start = (f32[88,512]{1,0:T(8,128)S(1)}, f32[88,512]{1,0:T(8,128)S(1)}, u32[]{:S(2)}, u32[]{:S(2)}) collective-permute-start(f32[88,512]{1,0:T(8,128)S(1)} %convert_element_type.3), channel_id=1, source_target_pairs={{0,8},{8,0},{64,72},{72,64},{1,9},{9,1},{65,73},{73,65},{2,10},{10... | collective-permute-start | bytes 540680 | tf_op jit(solution)/shard_map/ppermute | solution.py:129
  37.2 3.2 %collective-permute-start.1 = (f32[88,512]{1,0:T(8,128)S(1)}, f32[88,512]{1,0:T(8,128)S(1)}, u32[]{:S(2)}, u32[]{:S(2)}) collective-permute-start(f32[88,512]{1,0:T(8,128)S(1)} %convert_element_type.3), channel_id=1, source_target_pairs={{0,64},{8,72},{64,0},{72,8},{1,65},{9,73},{65,1},{73,9},{2,66},{10... | collective-permute-start | bytes 540680 | tf_op jit(solution)/shard_map/ppermute | solution.py:129
  40.4 1.9 %collective-permute-start.2 = (f32[88,512]{1,0:T(8,128)S(1)}, f32[88,512]{1,0:T(8,128)S(1)}, u32[]{:S(2)}, u32[]{:S(2)}) collective-permute-start(f32[88,512]{1,0:T(8,128)S(1)} %convert_element_type.3), channel_id=1, source_target_pairs={{0,72},{8,64},{64,8},{72,0},{1,73},{9,65},{65,9},{73,1},{2,74},{10... | collective-permute-start | bytes 540680 | tf_op jit(solution)/shard_map/ppermute | solution.py:129
  42.3 0.5 collective-permute-done.w1
  42.8 1.7 %collective-permute-done.1.w2 = f32[88,512]{1,0:T(8,128)S(1)} collective-permute-done((f32[88,512]{1,0:T(8,128)S(1)}, f32[88,512]{1,0:T(8,128)S(1)}, u32[]{:S(2)}, u32[]{:S(2)}) %collective-permute-start.1) | collective-permute-done | bytes 180256 | tf_op jit(solution)/shard_map/ppermute | solution.py:129
  44.5 3.8 %collective-permute-done.2.w3 = f32[88,512]{1,0:T(8,128)S(1)} collective-permute-done((f32[88,512]{1,0:T(8,128)S(1)}, f32[88,512]{1,0:T(8,128)S(1)}, u32[]{:S(2)}, u32[]{:S(2)}) %collective-permute-start.2) | collective-permute-done | bytes 180256 | tf_op jit(solution)/shard_map/ppermute | solution.py:129
  48.3 0.0 all-to-all-done.1
  48.3 1.0 %back.1 = f32[32,4,512]{2,1,0:T(4,128)} custom-call(s32[1]{0:T(128)} %bitcast.here, f32[4,128,88]{2,1,0:T(8,128)S(1)} %bitcast.5, bf16[88,512]{1,0:T(8,128)(2,1)S(1)} %copy-done, f32[88,512]{1,0:T(8,128)S(1)} %collective-permute-done.w1, f32[88,512]{1,0:T(8,128)S(1)} %collective-permute-done.1.w2, f32[88,512]{1,0:T(8,128)S(1)} %collective-permute-done.2.w3), custom_call_target="tpu_custom_call" | custom-call | tf_op jit(solution)/shard_map/back/pallas_call | solution.py:144
  49.3 12.4 %all-to-all-start.2 = ((f32[32,4,512]{2,1,0:T(4,128)}), f32[32,4,512]{2,1,0:T(4,128)S(1)}, u32[]{:S(2)}, u32[]{:S(2)}) async-start(f32[32,4,512]{2,1,0:T(4,128)} %back.1), calls=%async_computation.2 | async-start | bytes 524288 | tf_op jit(solution)/shard_map/all_to_all | solution.py:22
  61.8 0.0 copy-start.1
  61.8 0.7 copy-done.1
  62.5 0.7 constant_dynamic-slice_fusion.residual
  63.2 17.6 %all-to-all-done.2.sums = f32[32,4,512]{2,1,0:T(4,128)S(1)} async-done(((f32[32,4,512]{2,1,0:T(4,128)}), f32[32,4,512]{2,1,0:T(4,128)S(1)}, u32[]{:S(2)}, u32[]{:S(2)}) %all-to-all-start.2) | async-done | bytes 262176 | tf_op jit(solution)/shard_map/all_to_all | solution.py:22
  80.8 0.1 fold.1
  80.9 13.4 %all_to_all.21.sq = f32[8,4,128]{2,1,0:T(4,128)S(1)} all-to-all(f32[8,4,128]{2,1,0:T(4,128)S(1)} %get-tuple-element.8), channel_id=1, replica_groups=mesh['zq'=8,'z0'=2,'yq'=4,'y0'=2,'cb'=8] {'cb'}, dimensions={0} | all-to-all | bytes 32768 | tf_op jit(solution)/shard_map/all_to_all | solution.py:22
  94.3 0.7 finish.1
  (2 shorter events, 0.0 us)
Async XLA Ops:
  29.3 4.5 %copy-start = (bf16[88,512]{1,0:T(8,128)(2,1)S(1)}, bf16[88,512]{1,0:T(8,128)(2,1)}, u32[]{:S(2)}) copy-start(bf16[88,512]{1,0:T(8,128)(2,1)} %w0.1) | copy-start | bytes 270340
  29.3 19.0 %all-to-all-start.1 = ((f32[32,16,88]{2,1,0:T(8,128)}), f32[32,16,88]{2,1,0:T(8,128)S(1)}, u32[]{:S(2)}, u32[]{:S(2)}) async-start(f32[32,16,88]{2,1,0:T(8,128)} %bitcast.3), calls=%async_computation.1 | async-start | bytes 524288 | tf_op jit(solution)/shard_map/all_to_all | solution.py:22
  33.8 9.0 %collective-permute-start = (f32[88,512]{1,0:T(8,128)S(1)}, f32[88,512]{1,0:T(8,128)S(1)}, u32[]{:S(2)}, u32[]{:S(2)}) collective-permute-start(f32[88,512]{1,0:T(8,128)S(1)} %convert_element_type.3), channel_id=1, source_target_pairs={{0,8},{8,0},{64,72},{72,64},{1,9},{9,1},{65,73},{73,65},{2,10},{10... | collective-permute-start | bytes 540680 | tf_op jit(solution)/shard_map/ppermute | solution.py:129
  37.2 7.3 %collective-permute-start.1 = (f32[88,512]{1,0:T(8,128)S(1)}, f32[88,512]{1,0:T(8,128)S(1)}, u32[]{:S(2)}, u32[]{:S(2)}) collective-permute-start(f32[88,512]{1,0:T(8,128)S(1)} %convert_element_type.3), channel_id=1, source_target_pairs={{0,64},{8,72},{64,0},{72,8},{1,65},{9,73},{65,1},{73,9},{2,66},{10... | collective-permute-start | bytes 540680 | tf_op jit(solution)/shard_map/ppermute | solution.py:129
  40.4 8.0 %collective-permute-start.2 = (f32[88,512]{1,0:T(8,128)S(1)}, f32[88,512]{1,0:T(8,128)S(1)}, u32[]{:S(2)}, u32[]{:S(2)}) collective-permute-start(f32[88,512]{1,0:T(8,128)S(1)} %convert_element_type.3), channel_id=1, source_target_pairs={{0,72},{8,64},{64,8},{72,0},{1,73},{9,65},{65,9},{73,1},{2,74},{10... | collective-permute-start | bytes 540680 | tf_op jit(solution)/shard_map/ppermute | solution.py:129
  49.3 31.5 %all-to-all-start.2 = ((f32[32,4,512]{2,1,0:T(4,128)}), f32[32,4,512]{2,1,0:T(4,128)S(1)}, u32[]{:S(2)}, u32[]{:S(2)}) async-start(f32[32,4,512]{2,1,0:T(4,128)} %back.1), calls=%async_computation.2 | async-start | bytes 524288 | tf_op jit(solution)/shard_map/all_to_all | solution.py:22
  61.8 0.7 copy-start.1

commit v4 on v2

--- a/solution.py
+++ b/solution.py
@@ -22,28 +22,16 @@
     return lax.all_to_all(array, axes, split_axis=0, concat_axis=0, tiled=True)
 
 
-def copies(sources, targets, sems):
-    started = [pltpu.make_async_copy(s, t, sems.at[k]) for k, (s, t) in enumerate(zip(sources, targets))]
-    for c in started:
-        c.start()
-    return started
-
-
-def front(tok_hbm, gain_hbm, wg_hbm, wu_hbm, out, tok, gain, wg, wu, sems):
-    pending = copies((tok_hbm, gain_hbm, wg_hbm, wu_hbm), (tok, gain, wg, wu), sems)
+def front(tok, gain, wg, wu, out):
     n_cb, _, lanes = out.shape
     rows, cols = tok.shape
     units = wg.shape[0]
     share = rows // n_cb
     half = share // 2
     first = lanes - units
-    pending[0].wait()
-    pending[1].wait()
     x = tok[...].astype(F32)
     sq = jnp.sum(x * x, axis=1, keepdims=True)
     scaled = (x * gain[...].astype(F32).reshape(1, cols)).astype(BF16)
-    pending[2].wait()
-    pending[3].wait()
     up = wu[...].astype(F32)
     left = jnp.concatenate([wg[...].astype(F32), up[:first]], axis=0).astype(BF16)
     gap = jnp.zeros((lanes // 2 - (units - first), cols), F32)
@@ -87,7 +75,7 @@
                 out[a, b, j] = block
 
 
-def back(here, hid, w0, w1, w2, w3, out):
+def back(here, hid, w0, w1, w2, w3, _residual, _gain, out):
     acc = None
     for k, w in enumerate((w0, w1, w2, w3)):
         left = hid[here[0] ^ k].astype(BF16)
@@ -98,21 +86,16 @@
         out[k] = acc[k * per : (k + 1) * per]
 
 
-def fold(here, sums, tok, mixed, sq):
-    _, per, _ = sums.shape
-    down = jnp.sum(sums[...], axis=0)
-    pair = tok[...].astype(F32)
-    residual = jnp.where(here[1] % 2 == 1, pair[per:], pair[:per])
-    value = 0.1 * residual + down
-    mixed[...] = value
+def fold(sums, residual, gain, gained, sq):
+    value = 0.1 * residual[...].astype(F32) + jnp.sum(sums[...], axis=0)
+    gained[...] = value * gain[...].astype(F32)
     total = jnp.sum(value * value, axis=1, keepdims=True)
     sq[...] = jnp.broadcast_to(total[None], sq.shape)
 
 
-def finish(mixed, sq, gain, out):
+def finish(gained, sq, out):
     total = jnp.sum(sq[...], axis=0)[:, :1]
-    inv = lax.rsqrt(total / D + EPS)
-    out[...] = (mixed[...] * inv * gain[...].astype(F32)).astype(BF16)
+    out[...] = (gained[...] * lax.rsqrt(total / D + EPS)).astype(BF16)
 
 
 def body(tokens, norm_gain, w_gate, w_up, w_down, out_gain):
@@ -132,38 +115,31 @@
 
     lanes = 128
     packed = share + share // 2
-    partial = pl.pallas_call(
-        front, in_specs=[pl.BlockSpec(memory_space=pltpu.HBM)] * 4,
-        out_shape=jax.ShapeDtypeStruct((n_cb, packed, lanes), F32),
-        scratch_shapes=[pltpu.VMEM((rows, cols), BF16), pltpu.VMEM((cols,), BF16), pltpu.VMEM((units, cols), BF16),
-                        pltpu.VMEM((units, cols), BF16), pltpu.SemaphoreType.DMA((4,))],
-        name="front")(tokens, norm_gain, w_gate.T, w_up.T)
+    partial = pl.pallas_call(front, out_shape=jax.ShapeDtypeStruct((n_cb, packed, lanes), F32), name="front", compiler_params=SMALL)(
+        tokens, norm_gain, w_gate.T, w_up.T)
     parts = exchange(partial, "cb")
     blocks = pl.pallas_call(middle, out_shape=jax.ShapeDtypeStruct((2, 2, n_cb, held, units), F32), name="middle", compiler_params=SMALL)(parts)
     got = exchange(blocks.reshape(n_quad * n_cb, held, units), QUAD + ("cb",))
 
-    here = jnp.stack([lax.axis_index(QUAD), lax.axis_index(RA)]).astype(jnp.int32)
+    residual = lax.dynamic_slice_in_dim(tokens, lax.axis_index(RA) * own, own, 0)
+    wide_gain = out_gain.astype(F32)[None, :]
+    here = lax.axis_index(QUAD).astype(jnp.int32)[None]
     sums = pl.pallas_call(
         back,
         grid_spec=pltpu.PrefetchScalarGridSpec(num_scalar_prefetch=1, grid=(1,), in_specs=[
             pl.BlockSpec((n_quad, n_cb * held, units), lambda i, m: (0, 0, 0)),
             *[pl.BlockSpec((units, cols), lambda i, m: (0, 0))] * 4,
+            *[pl.BlockSpec(memory_space=pl.ANY)] * 2,
         ], out_specs=pl.BlockSpec((n_rest, own, cols), lambda i, m: (0, 0, 0))),
         out_shape=jax.ShapeDtypeStruct((n_rest, own, cols), F32), name="back", compiler_params=SMALL)(
-        here, got.reshape(n_quad, n_cb * held, units), w_down, *others)
+        here, got.reshape(n_quad, n_cb * held, units), w_down, *others, residual, wide_gain)
     sums = exchange(sums, REST)
 
-    mixed, sq = pl.pallas_call(
-        fold,
-        grid_spec=pltpu.PrefetchScalarGridSpec(num_scalar_prefetch=1, grid=(1,), in_specs=[
-            pl.BlockSpec((n_rest, own, cols), lambda i, m: (0, 0, 0)),
-            pl.BlockSpec((2 * own, cols), lambda i, m: (m[1] // 2, 0)),
-        ], out_specs=[pl.BlockSpec((own, cols), lambda i, m: (0, 0)), pl.BlockSpec((n_cb, own, 128), lambda i, m: (0, 0, 0))]),
-        out_shape=[jax.ShapeDtypeStruct((own, cols), F32), jax.ShapeDtypeStruct((n_cb, own, 128), F32)], name="fold", compiler_params=SMALL)(
-        here, sums, tokens)
+    gained, sq = pl.pallas_call(
+        fold, out_shape=[jax.ShapeDtypeStruct((own, cols), F32), jax.ShapeDtypeStruct((n_cb, own, 128), F32)], name="fold", compiler_params=SMALL)(
+        sums, residual, wide_gain)
     sq = exchange(sq, "cb")
-    return pl.pallas_call(finish, out_shape=jax.ShapeDtypeStruct((own, cols), BF16), name="finish", compiler_params=SMALL)(
-        mixed, sq, out_gain[None, :])
+    return pl.pallas_call(finish, out_shape=jax.ShapeDtypeStruct((own, cols), BF16), name="finish", compiler_params=SMALL)(gained, sq)
 
 
 def solution(mesh):

time: 96.4 us -> 95.6 us (level)
  blocking collectives: 56.9 us -> 70 us
  starting transfers between devices: 22 us -> 13 us
  waiting for transfers between devices: 10.6 us -> 4.63 us
  local copies, waits for them, and re-layouts: 0.02 us -> 4.88 us
  Pallas kernels: 6.17 us -> 2.45 us
    all_to_all x2 -> x3, blocking collectives: 56.9 us -> 70 us  [exchange(): return lax.all_to_all(array, axes, split_axis=0, concat_axis=0, tiled=True)]
    all_to_all x2 -> x1, starting transfers between devices: 13.6 us -> 4.52 us  [exchange(): return lax.all_to_all(array, axes, split_axis=0, concat_axis=0, tiled=True)]
    all_to_all x2 -> x1, waiting for transfers between devices: 4.65 us -> 0.01 us  [exchange(): return lax.all_to_all(array, axes, split_axis=0, concat_axis=0, tiled=True)]
    unnamed x6 -> x12, local copies, waits for them, and re-layouts: 0.01 us -> 4.18 us
    pallas_call x2, Pallas kernels: 3.77 us -> 0.58 us  [the longest x1 0.44 us: body(): pl.pallas_call(front, out_shape=jax.ShapeDtypeStruct((n_cb, packed, lanes...]
    ppermute x3, waiting for transfers between devices: 5.94 us -> 4.62 us  [body(): others.append(lax.ppermute(mine, QUAD, [(i, i ^ k) for i in range(n_quad)]))]
  transfers between devices with their start and end apart: 5 -> 4, of which waited for: 4 -> 2; matrix products, arithmetic and copies ran while one was open for 0% -> 1% of each run, Pallas kernels for 0% -> 0%
where the time goes in v4:
time: 95.6 us; the launch traced here: 95 us
  blocking collectives  70 us (73%)
  starting transfers between devices  13 us (14%)
  local copies, waits for them, and re-layouts  4.88 us (5%)
  waiting for transfers between devices  4.63 us (5%)
  Pallas kernels  2.45 us (3%)
    all_to_all x3, blocking collectives, exchange(): return lax.all_to_all(array, axes, split_axis=0, concat_axis=0, tiled=True)  70 us
    ppermute x3, starting transfers between devices, body(): others.append(lax.ppermute(mine, QUAD, [(i, i ^ k) for i in range(n_quad)]))  8.44 us
    ppermute x3, waiting for transfers between devices, body(): others.append(lax.ppermute(mine, QUAD, [(i, i ^ k) for i in range(n_quad)]))  4.62 us
    all_to_all x1, starting transfers between devices, exchange(): return lax.all_to_all(array, axes, split_axis=0, concat_axis=0, tiled=True)  4.52 us
    unnamed x12, local copies, waits for them, and re-layouts  4.18 us
  transfers between devices with their start and end apart: 4, of which 2 were waited for; matrix products, arithmetic and copies ran while one was open for 1% of the time, Pallas kernels for 0%

profile of v4, /device:TPU:1, one launch (start us, length us, event | category | flops | bytes accessed | tf_op | source)
XLA Modules:
  0.0 95.0 jit_solution(7266564344041272254)
XLA Ops:
  0.0 0.7 copy-done.4
  0.7 1.0 %copy-done = bf16[512,512]{1,0:T(8,128)(2,1)S(1)} copy-done((bf16[512,512]{1,0:T(8,128)(2,1)S(1)}, bf16[512,512]{1,0:T(8,128)(2,1)}, u32[]{:S(2)}) %copy-start) | copy-done | bytes 524312
  1.7 0.9 copy-done.2
  2.6 0.9 copy-done.3
  3.5 0.4 front.1
  4.0 24.5 %all_to_all.20.parts = f32[8,96,128]{2,1,0:T(8,128)S(1)} all-to-all(f32[8,96,128]{2,1,0:T(8,128)S(1)} %front.1), channel_id=1, replica_groups=mesh['zq'=8,'z0'=2,'yq'=4,'y0'=2,'cb'=8] {'cb'}, dimensions={0} | all-to-all | bytes 786432 | tf_op jit(solution)/shard_map/all_to_all | solution.py:22
  28.5 0.9 middle.1
  29.4 4.5 %all-to-all-start.1 = ((f32[32,16,88]{2,1,0:T(8,128)}), f32[32,16,88]{2,1,0:T(8,128)S(1)}, u32[]{:S(2)}, u32[]{:S(2)}) async-start(f32[32,16,88]{2,1,0:T(8,128)} %bitcast.3), calls=%async_computation.1 | async-start | bytes 524288 | tf_op jit(solution)/shard_map/all_to_all | solution.py:22
  33.9 0.0 copy-done.1
  34.0 3.3 %collective-permute-start = (f32[88,512]{1,0:T(8,128)S(1)}, f32[88,512]{1,0:T(8,128)S(1)}, u32[]{:S(2)}, u32[]{:S(2)}) collective-permute-start(f32[88,512]{1,0:T(8,128)S(1)} %convert_element_type.4), channel_id=1, source_target_pairs={{0,8},{8,0},{64,72},{72,64},{1,9},{9,1},{65,73},{73,65},{2,10},{10... | collective-permute-start | bytes 540680 | tf_op jit(solution)/shard_map/ppermute | solution.py:114
  37.3 3.2 %collective-permute-start.1 = (f32[88,512]{1,0:T(8,128)S(1)}, f32[88,512]{1,0:T(8,128)S(1)}, u32[]{:S(2)}, u32[]{:S(2)}) collective-permute-start(f32[88,512]{1,0:T(8,128)S(1)} %convert_element_type.4), channel_id=1, source_target_pairs={{0,64},{8,72},{64,0},{72,8},{1,65},{9,73},{65,1},{73,9},{2,66},{10... | collective-permute-start | bytes 540680 | tf_op jit(solution)/shard_map/ppermute | solution.py:114
  40.5 1.9 %collective-permute-start.2 = (f32[88,512]{1,0:T(8,128)S(1)}, f32[88,512]{1,0:T(8,128)S(1)}, u32[]{:S(2)}, u32[]{:S(2)}) collective-permute-start(f32[88,512]{1,0:T(8,128)S(1)} %convert_element_type.4), channel_id=1, source_target_pairs={{0,72},{8,64},{64,8},{72,0},{1,73},{9,65},{65,9},{73,1},{2,74},{10... | collective-permute-start | bytes 540680 | tf_op jit(solution)/shard_map/ppermute | solution.py:114
  42.4 0.0 copy-start.5
  42.4 0.7 copy-done.5
  43.1 0.7 constant_dynamic-slice_fusion._residual.residual
  43.8 0.0 collective-permute-done.w1
  43.8 0.8 collective-permute-done.1.w2
  44.6 3.8 %collective-permute-done.2.w3 = f32[88,512]{1,0:T(8,128)S(1)} collective-permute-done((f32[88,512]{1,0:T(8,128)S(1)}, f32[88,512]{1,0:T(8,128)S(1)}, u32[]{:S(2)}, u32[]{:S(2)}) %collective-permute-start.2) | collective-permute-done | bytes 180256 | tf_op jit(solution)/shard_map/ppermute | solution.py:114
  48.4 0.0 all-to-all-done.1
  48.4 0.3 back.1
  48.7 32.0 %all_to_all.21.sums = f32[32,4,512]{2,1,0:T(4,128)S(1)} all-to-all(f32[32,4,512]{2,1,0:T(4,128)S(1)} %back.1), channel_id=1, replica_groups=mesh['zq'=8,'z0'=2,'yq'=4,'y0'=2,'cb'=8] {'zq','yq'}, dimensions={0} | all-to-all | bytes 524288 | tf_op jit(solution)/shard_map/all_to_all | solution.py:22
  80.8 0.1 fold.1
  80.9 13.4 %all_to_all.22.sq = f32[8,4,128]{2,1,0:T(4,128)S(1)} all-to-all(f32[8,4,128]{2,1,0:T(4,128)S(1)} %get-tuple-element.8), channel_id=1, replica_groups=mesh['zq'=8,'z0'=2,'yq'=4,'y0'=2,'cb'=8] {'cb'}, dimensions={0} | all-to-all | bytes 32768 | tf_op jit(solution)/shard_map/all_to_all | solution.py:22
  94.3 0.7 finish.1
  (7 shorter events, 0.0 us)
Async XLA Ops:
  0.0 0.7 copy-start.4
  0.7 1.0 %copy-start = (bf16[512,512]{1,0:T(8,128)(2,1)S(1)}, bf16[512,512]{1,0:T(8,128)(2,1)}, u32[]{:S(2)}) copy-start(bf16[512,512]{1,0:T(8,128)(2,1)} %tok.1) | copy-start | bytes 1572868
  1.7 0.9 copy-start.2
  2.6 0.9 copy-start.3
  29.4 4.5 %copy-start.1 = (bf16[88,512]{1,0:T(8,128)(2,1)S(1)}, bf16[88,512]{1,0:T(8,128)(2,1)}, u32[]{:S(2)}) copy-start(bf16[88,512]{1,0:T(8,128)(2,1)} %w0.1) | copy-start | bytes 270340
  29.4 19.0 %all-to-all-start.1 = ((f32[32,16,88]{2,1,0:T(8,128)}), f32[32,16,88]{2,1,0:T(8,128)S(1)}, u32[]{:S(2)}, u32[]{:S(2)}) async-start(f32[32,16,88]{2,1,0:T(8,128)} %bitcast.3), calls=%async_computation.1 | async-start | bytes 524288 | tf_op jit(solution)/shard_map/all_to_all | solution.py:22
  34.0 9.9 %collective-permute-start = (f32[88,512]{1,0:T(8,128)S(1)}, f32[88,512]{1,0:T(8,128)S(1)}, u32[]{:S(2)}, u32[]{:S(2)}) collective-permute-start(f32[88,512]{1,0:T(8,128)S(1)} %convert_element_type.4), channel_id=1, source_target_pairs={{0,8},{8,0},{64,72},{72,64},{1,9},{9,1},{65,73},{73,65},{2,10},{10... | collective-permute-start | bytes 540680 | tf_op jit(solution)/shard_map/ppermute | solution.py:114
  37.3 7.3 %collective-permute-start.1 = (f32[88,512]{1,0:T(8,128)S(1)}, f32[88,512]{1,0:T(8,128)S(1)}, u32[]{:S(2)}, u32[]{:S(2)}) collective-permute-start(f32[88,512]{1,0:T(8,128)S(1)} %convert_element_type.4), channel_id=1, source_target_pairs={{0,64},{8,72},{64,0},{72,8},{1,65},{9,73},{65,1},{73,9},{2,66},{10... | collective-permute-start | bytes 540680 | tf_op jit(solution)/shard_map/ppermute | solution.py:114
  40.5 8.0 %collective-permute-start.2 = (f32[88,512]{1,0:T(8,128)S(1)}, f32[88,512]{1,0:T(8,128)S(1)}, u32[]{:S(2)}, u32[]{:S(2)}) collective-permute-start(f32[88,512]{1,0:T(8,128)S(1)} %convert_element_type.4), channel_id=1, source_target_pairs={{0,72},{8,64},{64,8},{72,0},{1,73},{9,65},{65,9},{73,1},{2,74},{10... | collective-permute-start | bytes 540680 | tf_op jit(solution)/shard_map/ppermute | solution.py:114
  42.4 0.7 copy-start.5

commit v5 on v4

--- a/solution.py
+++ b/solution.py
@@ -20,6 +20,26 @@
 
 def exchange(array, axes):
     return lax.all_to_all(array, axes, split_axis=0, concat_axis=0, tiled=True)
+
+
+def enter(here, down_hbm, tok_hbm, gain_hbm, wg_hbm, wu_hbm, last_hbm, wide, last, own, out, narrow, tok, gain, wg, wu, sems):
+    rows = own.shape[0]
+    source = tok_hbm.at[pl.ds(pl.multiple_of(here[0] // 2 * rows, rows), rows)]
+    pairs = ((down_hbm, narrow), (wg_hbm, wg), (wu_hbm, wu), (gain_hbm, gain), (tok_hbm, tok), (last_hbm, last), (source, own))
+    pending = [pltpu.make_async_copy(a, b, sems.at[k]) for k, (a, b) in enumerate(pairs)]
+    for c in pending:
+        c.start()
+    pending[0].wait()
+    wide[...] = narrow[...].astype(F32)
+    for c in pending[1:]:
+        c.wait()
+    front(tok, gain, wg, wu, out)
+
+
+def order(here, hid, out):
+    quad = here[0] // 8 % 2 * 2 + here[0] % 2
+    for k in range(out.shape[0]):
+        out[k] = hid[quad ^ k].astype(BF16)
 
 
 def front(tok, gain, wg, wu, out):
@@ -75,20 +95,21 @@
                 out[a, b, j] = block
 
 
-def back(here, hid, w0, w1, w2, w3, _residual, _gain, out):
+def back(hid, w0, w1, w2, w3, out):
     acc = None
     for k, w in enumerate((w0, w1, w2, w3)):
-        left = hid[here[0] ^ k].astype(BF16)
-        part = jnp.dot(left, w[...].astype(BF16), preferred_element_type=F32)
+        part = jnp.dot(hid[k], w[...].astype(BF16), preferred_element_type=F32)
         acc = part if acc is None else acc + part
     n, per, _ = out.shape
     for k in range(n):
         out[k] = acc[k * per : (k + 1) * per]
 
 
-def fold(sums, residual, gain, gained, sq):
-    value = 0.1 * residual[...].astype(F32) + jnp.sum(sums[...], axis=0)
-    gained[...] = value * gain[...].astype(F32)
+def fold(here, sums, residual, gain, gained, sq):
+    per, cols = gained.shape
+    pair = residual[...].astype(F32)
+    value = 0.1 * jnp.where(here[0] % 2 == 1, pair[per:], pair[:per]) + jnp.sum(sums[...], axis=0)
+    gained[...] = value * gain[...].astype(F32).reshape(1, cols)
     total = jnp.sum(value * value, axis=1, keepdims=True)
     sq[...] = jnp.broadcast_to(total[None], sq.shape)
 
@@ -108,36 +129,50 @@
     share = rows // n_cb
     held = share // n_quad
 
-    mine = w_down.astype(F32)
+    here = lax.axis_index(RA).astype(jnp.int32)[None]
+    lanes = 128
+    packed = share + share // 2
+    inputs = (w_down, tokens, norm_gain, w_gate.T, w_up.T, out_gain)
+    hbm = [pltpu.with_memory_space_constraint(x, pltpu.HBM) for x in inputs]
+    whole = lambda *shape: pl.BlockSpec(shape, lambda i, m: (0,) * len(shape))
+    mine, out_gain, residual, partial = pl.pallas_call(
+        enter,
+        grid_spec=pltpu.PrefetchScalarGridSpec(
+            num_scalar_prefetch=1, grid=(1,), in_specs=[pl.BlockSpec(memory_space=pltpu.HBM)] * 6,
+            out_specs=[whole(units, cols), whole(cols), whole(2 * own, cols), whole(n_cb, packed, lanes)],
+            scratch_shapes=[pltpu.VMEM((units, cols), BF16), pltpu.VMEM((rows, cols), BF16), pltpu.VMEM((cols,), BF16),
+                            pltpu.VMEM((units, cols), BF16), pltpu.VMEM((units, cols), BF16), pltpu.SemaphoreType.DMA((7,))]),
+        out_shape=[jax.ShapeDtypeStruct((units, cols), F32), jax.ShapeDtypeStruct((cols,), BF16), jax.ShapeDtypeStruct((2 * own, cols), BF16),
+                   jax.ShapeDtypeStruct((n_cb, packed, lanes), F32)],
+        name="enter", compiler_params=SMALL)(here, *hbm)
     others = []
     for k in range(1, n_quad):
         others.append(lax.ppermute(mine, QUAD, [(i, i ^ k) for i in range(n_quad)]))
 
-    lanes = 128
-    packed = share + share // 2
-    partial = pl.pallas_call(front, out_shape=jax.ShapeDtypeStruct((n_cb, packed, lanes), F32), name="front", compiler_params=SMALL)(
-        tokens, norm_gain, w_gate.T, w_up.T)
     parts = exchange(partial, "cb")
     blocks = pl.pallas_call(middle, out_shape=jax.ShapeDtypeStruct((2, 2, n_cb, held, units), F32), name="middle", compiler_params=SMALL)(parts)
     got = exchange(blocks.reshape(n_quad * n_cb, held, units), QUAD + ("cb",))
 
-    residual = lax.dynamic_slice_in_dim(tokens, lax.axis_index(RA) * own, own, 0)
-    wide_gain = out_gain.astype(F32)[None, :]
-    here = lax.axis_index(QUAD).astype(jnp.int32)[None]
-    sums = pl.pallas_call(
-        back,
-        grid_spec=pltpu.PrefetchScalarGridSpec(num_scalar_prefetch=1, grid=(1,), in_specs=[
-            pl.BlockSpec((n_quad, n_cb * held, units), lambda i, m: (0, 0, 0)),
-            *[pl.BlockSpec((units, cols), lambda i, m: (0, 0))] * 4,
-            *[pl.BlockSpec(memory_space=pl.ANY)] * 2,
-        ], out_specs=pl.BlockSpec((n_rest, own, cols), lambda i, m: (0, 0, 0))),
-        out_shape=jax.ShapeDtypeStruct((n_rest, own, cols), F32), name="back", compiler_params=SMALL)(
-        here, got.reshape(n_quad, n_cb * held, units), w_down, *others, residual, wide_gain)
+    hidden = pl.pallas_call(
+        order,
+        grid_spec=pltpu.PrefetchScalarGridSpec(
+            num_scalar_prefetch=1, grid=(1,), in_specs=[pl.BlockSpec((n_quad, n_cb * held, units), lambda i, m: (0, 0, 0))],
+            out_specs=pl.BlockSpec((n_quad, n_cb * held, units), lambda i, m: (0, 0, 0))),
+        out_shape=jax.ShapeDtypeStruct((n_quad, n_cb * held, units), BF16), name="order", compiler_params=SMALL)(
+        here, got.reshape(n_quad, n_cb * held, units))
+    sums = pl.pallas_call(back, out_shape=jax.ShapeDtypeStruct((n_rest, own, cols), F32), name="back", compiler_params=SMALL)(
+        hidden, mine, *others)
     sums = exchange(sums, REST)
 
     gained, sq = pl.pallas_call(
-        fold, out_shape=[jax.ShapeDtypeStruct((own, cols), F32), jax.ShapeDtypeStruct((n_cb, own, 128), F32)], name="fold", compiler_params=SMALL)(
-        sums, residual, wide_gain)
+        fold,
+        grid_spec=pltpu.PrefetchScalarGridSpec(
+            num_scalar_prefetch=1, grid=(1,), in_specs=[
+                pl.BlockSpec((n_rest, own, cols), lambda i, m: (0, 0, 0)), pl.BlockSpec((2 * own, cols), lambda i, m: (0, 0)),
+                pl.BlockSpec((cols,), lambda i, m: (0,))],
+            out_specs=[pl.BlockSpec((own, cols), lambda i, m: (0, 0)), pl.BlockSpec((n_cb, own, 128), lambda i, m: (0, 0, 0))]),
+        out_shape=[jax.ShapeDtypeStruct((own, cols), F32), jax.ShapeDtypeStruct((n_cb, own, 128), F32)], name="fold", compiler_params=SMALL)(
+        here, sums, residual, out_gain)
     sq = exchange(sq, "cb")
     return pl.pallas_call(finish, out_shape=jax.ShapeDtypeStruct((own, cols), BF16), name="finish", compiler_params=SMALL)(gained, sq)
 

time: 95.6 us -> 92.1 us (0.963)
  local copies, waits for them, and re-layouts: 4.88 us -> 0 us
  Pallas kernels: 2.45 us -> 3.72 us
    unnamed x12 -> x0, local copies, waits for them, and re-layouts: 4.18 us -> none
    pallas_call x3 -> x4, Pallas kernels: 0.87 us -> 2.15 us  [the longest x1 1.71 us: body(): pl.pallas_call(enter, grid_spec=pltpu.PrefetchScalarGridSpec(num_scalar_p...]
  transfers between devices with their start and end apart: 4 -> 4, of which waited for: 2 -> 4; matrix products, arithmetic and copies ran while one was open for 1% -> 0% of each run, Pallas kernels for 0% -> 0%
where the time goes in v5:
time: 92.1 us; the launch traced here: 91.7 us
  blocking collectives  70.1 us (76%)
  starting transfers between devices  12.8 us (14%)
  waiting for transfers between devices  4.99 us (5%)
  Pallas kernels  3.72 us (4%)
    all_to_all x3, blocking collectives, exchange(): return lax.all_to_all(array, axes, split_axis=0, concat_axis=0, tiled=True)  70.1 us
    ppermute x3, starting transfers between devices, body(): others.append(lax.ppermute(mine, QUAD, [(i, i ^ k) for i in range(n_quad)]))  8.44 us
    ppermute x3, waiting for transfers between devices, body(): others.append(lax.ppermute(mine, QUAD, [(i, i ^ k) for i in range(n_quad)]))  4.64 us
    all_to_all x1, starting transfers between devices, exchange(): return lax.all_to_all(array, axes, split_axis=0, concat_axis=0, tiled=True)  4.38 us
  transfers between devices with their start and end apart: 4, of which 4 were waited for; matrix products, arithmetic and copies ran while one was open for 0% of the time, Pallas kernels for 0%

profile of v5, /device:TPU:1, one launch (start us, length us, event | category | flops | bytes accessed | tf_op | source)
XLA Modules:
  0.0 91.7 jit_solution(13592489176567258836)
XLA Ops:
  0.0 1.7 %enter.1 = (f32[88,512]{1,0:T(8,128)S(1)}, bf16[512]{0:T(512)(128)(2,1)S(1)}, bf16[8,512]{1,0:T(8,128)(2,1)S(1)}, f32[8,96,128]{2,1,0:T(8,128)S(1)}) custom-call(s32[1]{0:T(128)} %bitcast.here, bf16[88,512]{1,0:T(8,128)(2,1)} %down_hbm.1, bf16[512,512]{1,0:T(8,128)(2,1)} %tok_hbm.1, bf16[512]{0:T(512)(128)(2,1)} %gain_hbm.1, bf16[88,512]{1,0:T(8,128)(2,1)} %bitcast.6, ...), custom_call_target="tpu_custom_call" | custom-call | tf_op jit(solution)/shard_map/enter/pallas_call | solution.py:138
  1.7 24.5 %all_to_all.20.parts = f32[8,96,128]{2,1,0:T(8,128)S(1)} all-to-all(f32[8,96,128]{2,1,0:T(8,128)S(1)} %get-tuple-element.11), channel_id=1, replica_groups=mesh['zq'=8,'z0'=2,'yq'=4,'y0'=2,'cb'=8] {'cb'}, dimensions={0} | all-to-all | bytes 786432 | tf_op jit(solution)/shard_map/all_to_all | solution.py:22
  26.3 0.9 middle.1
  27.2 4.4 %all-to-all-start.1 = ((f32[32,16,88]{2,1,0:T(8,128)}), f32[32,16,88]{2,1,0:T(8,128)S(1)}, u32[]{:S(2)}, u32[]{:S(2)}) async-start(f32[32,16,88]{2,1,0:T(8,128)} %bitcast.3), calls=%async_computation.1 | async-start | bytes 524288 | tf_op jit(solution)/shard_map/all_to_all | solution.py:22
  31.6 4.3 %collective-permute-start.2 = (f32[88,512]{1,0:T(8,128)S(1)}, f32[88,512]{1,0:T(8,128)S(1)}, u32[]{:S(2)}, u32[]{:S(2)}) collective-permute-start(f32[88,512]{1,0:T(8,128)S(1)} %get-tuple-element.12.w0), channel_id=1, source_target_pairs={{0,72},{8,64},{64,8},{72,0},{1,73},{9,65},{65,9},{73,1},{2,74},{10... | collective-permute-start | bytes 540680 | tf_op jit(solution)/shard_map/ppermute | solution.py:150
  35.9 2.1 %collective-permute-start.1 = (f32[88,512]{1,0:T(8,128)S(1)}, f32[88,512]{1,0:T(8,128)S(1)}, u32[]{:S(2)}, u32[]{:S(2)}) collective-permute-start(f32[88,512]{1,0:T(8,128)S(1)} %get-tuple-element.12.w0), channel_id=1, source_target_pairs={{0,64},{8,72},{64,0},{72,8},{1,65},{9,73},{65,1},{73,9},{2,66},{10... | collective-permute-start | bytes 540680 | tf_op jit(solution)/shard_map/ppermute | solution.py:150
  38.0 2.0 %collective-permute-start = (f32[88,512]{1,0:T(8,128)S(1)}, f32[88,512]{1,0:T(8,128)S(1)}, u32[]{:S(2)}, u32[]{:S(2)}) collective-permute-start(f32[88,512]{1,0:T(8,128)S(1)} %get-tuple-element.12.w0), channel_id=1, source_target_pairs={{0,8},{8,0},{64,72},{72,64},{1,9},{9,1},{65,73},{73,65},{2,10},{10... | collective-permute-start | bytes 540680 | tf_op jit(solution)/shard_map/ppermute | solution.py:150
  40.0 0.3 all-to-all-done.1
  40.4 1.0 %collective-permute-done.2.w3 = f32[88,512]{1,0:T(8,128)S(1)} collective-permute-done((f32[88,512]{1,0:T(8,128)S(1)}, f32[88,512]{1,0:T(8,128)S(1)}, u32[]{:S(2)}, u32[]{:S(2)}) %collective-permute-start.2) | collective-permute-done | bytes 180256 | tf_op jit(solution)/shard_map/ppermute | solution.py:150
  41.4 2.9 %collective-permute-done.1.w2 = f32[88,512]{1,0:T(8,128)S(1)} collective-permute-done((f32[88,512]{1,0:T(8,128)S(1)}, f32[88,512]{1,0:T(8,128)S(1)}, u32[]{:S(2)}, u32[]{:S(2)}) %collective-permute-start.1) | collective-permute-done | bytes 180256 | tf_op jit(solution)/shard_map/ppermute | solution.py:150
  44.3 0.7 collective-permute-done.w1
  45.0 0.3 back.1
  45.3 31.6 %all_to_all.21.sums = f32[32,4,512]{2,1,0:T(4,128)S(1)} all-to-all(f32[32,4,512]{2,1,0:T(4,128)S(1)} %back.1), channel_id=1, replica_groups=mesh['zq'=8,'z0'=2,'yq'=4,'y0'=2,'cb'=8] {'zq','yq'}, dimensions={0} | all-to-all | bytes 524288 | tf_op jit(solution)/shard_map/all_to_all | solution.py:22
  76.9 0.1 fold.1
  77.1 14.0 %all_to_all.22.sq = f32[8,4,128]{2,1,0:T(4,128)S(1)} all-to-all(f32[8,4,128]{2,1,0:T(4,128)S(1)} %get-tuple-element.16), channel_id=1, replica_groups=mesh['zq'=8,'z0'=2,'yq'=4,'y0'=2,'cb'=8] {'cb'}, dimensions={0} | all-to-all | bytes 32768 | tf_op jit(solution)/shard_map/all_to_all | solution.py:22
  91.0 0.7 finish.1
  (1 shorter events, 0.0 us)
Async XLA Ops:
  27.2 13.2 %all-to-all-start.1 = ((f32[32,16,88]{2,1,0:T(8,128)}), f32[32,16,88]{2,1,0:T(8,128)S(1)}, u32[]{:S(2)}, u32[]{:S(2)}) async-start(f32[32,16,88]{2,1,0:T(8,128)} %bitcast.3), calls=%async_computation.1 | async-start | bytes 524288 | tf_op jit(solution)/shard_map/all_to_all | solution.py:22
  31.6 9.9 %collective-permute-start.2 = (f32[88,512]{1,0:T(8,128)S(1)}, f32[88,512]{1,0:T(8,128)S(1)}, u32[]{:S(2)}, u32[]{:S(2)}) collective-permute-start(f32[88,512]{1,0:T(8,128)S(1)} %get-tuple-element.12.w0), channel_id=1, source_target_pairs={{0,72},{8,64},{64,8},{72,0},{1,73},{9,65},{65,9},{73,1},{2,74},{10... | collective-permute-start | bytes 540680 | tf_op jit(solution)/shard_map/ppermute | solution.py:150
  35.9 8.5 %collective-permute-start.1 = (f32[88,512]{1,0:T(8,128)S(1)}, f32[88,512]{1,0:T(8,128)S(1)}, u32[]{:S(2)}, u32[]{:S(2)}) collective-permute-start(f32[88,512]{1,0:T(8,128)S(1)} %get-tuple-element.12.w0), channel_id=1, source_target_pairs={{0,64},{8,72},{64,0},{72,8},{1,65},{9,73},{65,1},{73,9},{2,66},{10... | collective-permute-start | bytes 540680 | tf_op jit(solution)/shard_map/ppermute | solution.py:150
  38.0 7.1 %collective-permute-start = (f32[88,512]{1,0:T(8,128)S(1)}, f32[88,512]{1,0:T(8,128)S(1)}, u32[]{:S(2)}, u32[]{:S(2)}) collective-permute-start(f32[88,512]{1,0:T(8,128)S(1)} %get-tuple-element.12.w0), channel_id=1, source_target_pairs={{0,8},{8,0},{64,72},{72,64},{1,9},{9,1},{65,73},{73,65},{2,10},{10... | collective-permute-start | bytes 540680 | tf_op jit(solution)/shard_map/ppermute | solution.py:150

commit v6 on v5

--- a/solution.py
+++ b/solution.py
@@ -39,7 +39,9 @@
 def order(here, hid, out):
     quad = here[0] // 8 % 2 * 2 + here[0] % 2
     for k in range(out.shape[0]):
-        out[k] = hid[quad ^ k].astype(BF16)
+        for j in range(hid.shape[0]):
+            held = hid.shape[2]
+            out[k, j * held : (j + 1) * held] = hid[j, quad ^ k].astype(BF16)
 
 
 def front(tok, gain, wg, wu, out):
@@ -72,7 +74,7 @@
 
 
 def middle(parts, out):
-    n_z0, n_y0, n_cb, held, units = out.shape
+    n_cb, n_z0, n_y0, held, units = out.shape
     lanes = parts.shape[2]
     share = held * n_z0 * n_y0
     first = lanes - units
@@ -92,7 +94,7 @@
             rows = [((a * n_yq + q) * n_y0 + b) * r for q in range(n_yq)]
             block = jnp.concatenate([hidden[s : s + r] for s in rows], axis=0)
             for j in range(n_cb):
-                out[a, b, j] = block
+                out[j, a, b] = block
 
 
 def back(hid, w0, w1, w2, w3, out):
@@ -150,16 +152,16 @@
         others.append(lax.ppermute(mine, QUAD, [(i, i ^ k) for i in range(n_quad)]))
 
     parts = exchange(partial, "cb")
-    blocks = pl.pallas_call(middle, out_shape=jax.ShapeDtypeStruct((2, 2, n_cb, held, units), F32), name="middle", compiler_params=SMALL)(parts)
-    got = exchange(blocks.reshape(n_quad * n_cb, held, units), QUAD + ("cb",))
+    blocks = pl.pallas_call(middle, out_shape=jax.ShapeDtypeStruct((n_cb, 2, 2, held, units), F32), name="middle", compiler_params=SMALL)(parts)
+    got = exchange(blocks.reshape(n_quad * n_cb, held, units), ("cb",) + QUAD)
 
     hidden = pl.pallas_call(
         order,
         grid_spec=pltpu.PrefetchScalarGridSpec(
-            num_scalar_prefetch=1, grid=(1,), in_specs=[pl.BlockSpec((n_quad, n_cb * held, units), lambda i, m: (0, 0, 0))],
+            num_scalar_prefetch=1, grid=(1,), in_specs=[pl.BlockSpec((n_cb, n_quad, held, units), lambda i, m: (0, 0, 0, 0))],
             out_specs=pl.BlockSpec((n_quad, n_cb * held, units), lambda i, m: (0, 0, 0))),
         out_shape=jax.ShapeDtypeStruct((n_quad, n_cb * held, units), BF16), name="order", compiler_params=SMALL)(
-        here, got.reshape(n_quad, n_cb * held, units))
+        here, got.reshape(n_cb, n_quad, held, units))
     sums = pl.pallas_call(back, out_shape=jax.ShapeDtypeStruct((n_rest, own, cols), F32), name="back", compiler_params=SMALL)(
         hidden, mine, *others)
     sums = exchange(sums, REST)

time: 92.1 us -> 92.1 us (level)
  transfers between devices with their start and end apart: 4 -> 4, of which waited for: 4 -> 3; matrix products, arithmetic and copies ran while one was open for 0% -> 0% of each run, Pallas kernels for 0% -> 0%
where the time goes in v6:
time: 92.1 us; the launch traced here: 91.7 us
  blocking collectives  70.2 us (76%)
  starting transfers between devices  12.8 us (14%)
  waiting for transfers between devices  5 us (5%)
  Pallas kernels  3.74 us (4%)
    all_to_all x3, blocking collectives, exchange(): return lax.all_to_all(array, axes, split_axis=0, concat_axis=0, tiled=True)  70.2 us
    ppermute x3, starting transfers between devices, body(): others.append(lax.ppermute(mine, QUAD, [(i, i ^ k) for i in range(n_quad)]))  8.37 us
    ppermute x3, waiting for transfers between devices, body(): others.append(lax.ppermute(mine, QUAD, [(i, i ^ k) for i in range(n_quad)]))  5 us
    all_to_all x1, starting transfers between devices, exchange(): return lax.all_to_all(array, axes, split_axis=0, concat_axis=0, tiled=True)  4.41 us
  transfers between devices with their start and end apart: 4, of which 3 were waited for; matrix products, arithmetic and copies ran while one was open for 0% of the time, Pallas kernels for 0%

profile of v6, /device:TPU:1, one launch (start us, length us, event | category | flops | bytes accessed | tf_op | source)
XLA Modules:
  0.0 91.7 jit_solution(5910719843304797005)
XLA Ops:
  0.0 1.7 %enter.1 = (f32[88,512]{1,0:T(8,128)S(1)}, bf16[512]{0:T(512)(128)(2,1)S(1)}, bf16[8,512]{1,0:T(8,128)(2,1)S(1)}, f32[8,96,128]{2,1,0:T(8,128)S(1)}) custom-call(s32[1]{0:T(128)} %bitcast.here, bf16[88,512]{1,0:T(8,128)(2,1)} %down_hbm.1, bf16[512,512]{1,0:T(8,128)(2,1)} %tok_hbm.1, bf16[512]{0:T(512)(128)(2,1)} %gain_hbm.1, bf16[88,512]{1,0:T(8,128)(2,1)} %bitcast.6, ...), custom_call_target="tpu_custom_call" | custom-call | tf_op jit(solution)/shard_map/enter/pallas_call | solution.py:140
  1.7 24.5 %all_to_all.20.parts = f32[8,96,128]{2,1,0:T(8,128)S(1)} all-to-all(f32[8,96,128]{2,1,0:T(8,128)S(1)} %get-tuple-element.11), channel_id=1, replica_groups=mesh['zq'=8,'z0'=2,'yq'=4,'y0'=2,'cb'=8] {'cb'}, dimensions={0} | all-to-all | bytes 786432 | tf_op jit(solution)/shard_map/all_to_all | solution.py:22
  26.3 0.9 middle.1
  27.2 4.4 %all-to-all-start.1 = ((f32[32,16,88]{2,1,0:T(8,128)}), f32[32,16,88]{2,1,0:T(8,128)S(1)}, u32[]{:S(2)}, u32[]{:S(2)}) async-start(f32[32,16,88]{2,1,0:T(8,128)} %bitcast.3), calls=%async_computation.1 | async-start | bytes 524288 | tf_op jit(solution)/shard_map/all_to_all | solution.py:22
  31.6 4.2 %collective-permute-start.2 = (f32[88,512]{1,0:T(8,128)S(1)}, f32[88,512]{1,0:T(8,128)S(1)}, u32[]{:S(2)}, u32[]{:S(2)}) collective-permute-start(f32[88,512]{1,0:T(8,128)S(1)} %get-tuple-element.12.w0), channel_id=1, source_target_pairs={{0,72},{8,64},{64,8},{72,0},{1,73},{9,65},{65,9},{73,1},{2,74},{10... | collective-permute-start | bytes 540680 | tf_op jit(solution)/shard_map/ppermute | solution.py:152
  35.8 2.2 %collective-permute-start.1 = (f32[88,512]{1,0:T(8,128)S(1)}, f32[88,512]{1,0:T(8,128)S(1)}, u32[]{:S(2)}, u32[]{:S(2)}) collective-permute-start(f32[88,512]{1,0:T(8,128)S(1)} %get-tuple-element.12.w0), channel_id=1, source_target_pairs={{0,64},{8,72},{64,0},{72,8},{1,65},{9,73},{65,1},{73,9},{2,66},{10... | collective-permute-start | bytes 540680 | tf_op jit(solution)/shard_map/ppermute | solution.py:152
  37.9 2.0 %collective-permute-start = (f32[88,512]{1,0:T(8,128)S(1)}, f32[88,512]{1,0:T(8,128)S(1)}, u32[]{:S(2)}, u32[]{:S(2)}) collective-permute-start(f32[88,512]{1,0:T(8,128)S(1)} %get-tuple-element.12.w0), channel_id=1, source_target_pairs={{0,8},{8,0},{64,72},{72,64},{1,9},{9,1},{65,73},{73,65},{2,10},{10... | collective-permute-start | bytes 540680 | tf_op jit(solution)/shard_map/ppermute | solution.py:152
  40.0 0.0 all-to-all-done.1
  40.0 1.3 %collective-permute-done.2.w3 = f32[88,512]{1,0:T(8,128)S(1)} collective-permute-done((f32[88,512]{1,0:T(8,128)S(1)}, f32[88,512]{1,0:T(8,128)S(1)}, u32[]{:S(2)}, u32[]{:S(2)}) %collective-permute-start.2) | collective-permute-done | bytes 180256 | tf_op jit(solution)/shard_map/ppermute | solution.py:152
  41.3 2.9 %collective-permute-done.1.w2 = f32[88,512]{1,0:T(8,128)S(1)} collective-permute-done((f32[88,512]{1,0:T(8,128)S(1)}, f32[88,512]{1,0:T(8,128)S(1)}, u32[]{:S(2)}, u32[]{:S(2)}) %collective-permute-start.1) | collective-permute-done | bytes 180256 | tf_op jit(solution)/shard_map/ppermute | solution.py:152
  44.2 0.8 collective-permute-done.w1
  45.0 0.3 back.1
  45.3 31.6 %all_to_all.21.sums = f32[32,4,512]{2,1,0:T(4,128)S(1)} all-to-all(f32[32,4,512]{2,1,0:T(4,128)S(1)} %back.1), channel_id=1, replica_groups=mesh['zq'=8,'z0'=2,'yq'=4,'y0'=2,'cb'=8] {'zq','yq'}, dimensions={0} | all-to-all | bytes 524288 | tf_op jit(solution)/shard_map/all_to_all | solution.py:22
  76.9 0.1 fold.1
  77.1 14.0 %all_to_all.22.sq = f32[8,4,128]{2,1,0:T(4,128)S(1)} all-to-all(f32[8,4,128]{2,1,0:T(4,128)S(1)} %get-tuple-element.16), channel_id=1, replica_groups=mesh['zq'=8,'z0'=2,'yq'=4,'y0'=2,'cb'=8] {'cb'}, dimensions={0} | all-to-all | bytes 32768 | tf_op jit(solution)/shard_map/all_to_all | solution.py:22
  91.1 0.7 finish.1
  (1 shorter events, 0.0 us)
Async XLA Ops:
  27.2 12.8 %all-to-all-start.1 = ((f32[32,16,88]{2,1,0:T(8,128)}), f32[32,16,88]{2,1,0:T(8,128)S(1)}, u32[]{:S(2)}, u32[]{:S(2)}) async-start(f32[32,16,88]{2,1,0:T(8,128)} %bitcast.3), calls=%async_computation.1 | async-start | bytes 524288 | tf_op jit(solution)/shard_map/all_to_all | solution.py:22
  31.6 9.7 %collective-permute-start.2 = (f32[88,512]{1,0:T(8,128)S(1)}, f32[88,512]{1,0:T(8,128)S(1)}, u32[]{:S(2)}, u32[]{:S(2)}) collective-permute-start(f32[88,512]{1,0:T(8,128)S(1)} %get-tuple-element.12.w0), channel_id=1, source_target_pairs={{0,72},{8,64},{64,8},{72,0},{1,73},{9,65},{65,9},{73,1},{2,74},{10... | collective-permute-start | bytes 540680 | tf_op jit(solution)/shard_map/ppermute | solution.py:152
  35.8 8.5 %collective-permute-start.1 = (f32[88,512]{1,0:T(8,128)S(1)}, f32[88,512]{1,0:T(8,128)S(1)}, u32[]{:S(2)}, u32[]{:S(2)}) collective-permute-start(f32[88,512]{1,0:T(8,128)S(1)} %get-tuple-element.12.w0), channel_id=1, source_target_pairs={{0,64},{8,72},{64,0},{72,8},{1,65},{9,73},{65,1},{73,9},{2,66},{10... | collective-permute-start | bytes 540680 | tf_op jit(solution)/shard_map/ppermute | solution.py:152
  37.9 7.1 %collective-permute-start = (f32[88,512]{1,0:T(8,128)S(1)}, f32[88,512]{1,0:T(8,128)S(1)}, u32[]{:S(2)}, u32[]{:S(2)}) collective-permute-start(f32[88,512]{1,0:T(8,128)S(1)} %get-tuple-element.12.w0), channel_id=1, source_target_pairs={{0,8},{8,0},{64,72},{72,64},{1,9},{9,1},{65,73},{73,65},{2,10},{10... | collective-permute-start | bytes 540680 | tf_op jit(solution)/shard_map/ppermute | solution.py:152

commit v7 on v6

--- a/solution.py
+++ b/solution.py
@@ -102,15 +102,19 @@
     for k, w in enumerate((w0, w1, w2, w3)):
         part = jnp.dot(hid[k], w[...].astype(BF16), preferred_element_type=F32)
         acc = part if acc is None else acc + part
-    n, per, _ = out.shape
+    n, held, lanes = out.shape
+    blocks = acc.shape[1] // lanes
+    per = held // blocks
     for k in range(n):
-        out[k] = acc[k * per : (k + 1) * per]
+        out[k] = jnp.concatenate([acc[k * per : (k + 1) * per, b * lanes : (b + 1) * lanes] for b in range(blocks)], axis=0)
 
 
 def fold(here, sums, residual, gain, gained, sq):
     per, cols = gained.shape
     pair = residual[...].astype(F32)
-    value = 0.1 * jnp.where(here[0] % 2 == 1, pair[per:], pair[:per]) + jnp.sum(sums[...], axis=0)
+    down = jnp.sum(sums[...], axis=0)
+    down = jnp.concatenate([down[b * per : (b + 1) * per] for b in range(down.shape[0] // per)], axis=1)
+    value = 0.1 * jnp.where(here[0] % 2 == 1, pair[per:], pair[:per]) + down
     gained[...] = value * gain[...].astype(F32).reshape(1, cols)
     total = jnp.sum(value * value, axis=1, keepdims=True)
     sq[...] = jnp.broadcast_to(total[None], sq.shape)
@@ -162,7 +166,7 @@
             out_specs=pl.BlockSpec((n_quad, n_cb * held, units), lambda i, m: (0, 0, 0))),
         out_shape=jax.ShapeDtypeStruct((n_quad, n_cb * held, units), BF16), name="order", compiler_params=SMALL)(
         here, got.reshape(n_cb, n_quad, held, units))
-    sums = pl.pallas_call(back, out_shape=jax.ShapeDtypeStruct((n_rest, own, cols), F32), name="back", compiler_params=SMALL)(
+    sums = pl.pallas_call(back, out_shape=jax.ShapeDtypeStruct((n_rest, own * cols // 128, 128), F32), name="back", compiler_params=SMALL)(
         hidden, mine, *others)
     sums = exchange(sums, REST)
 
@@ -170,7 +174,7 @@
         fold,
         grid_spec=pltpu.PrefetchScalarGridSpec(
             num_scalar_prefetch=1, grid=(1,), in_specs=[
-                pl.BlockSpec((n_rest, own, cols), lambda i, m: (0, 0, 0)), pl.BlockSpec((2 * own, cols), lambda i, m: (0, 0)),
+                pl.BlockSpec((n_rest, own * cols // 128, 128), lambda i, m: (0, 0, 0)), pl.BlockSpec((2 * own, cols), lambda i, m: (0, 0)),
                 pl.BlockSpec((cols,), lambda i, m: (0,))],
             out_specs=[pl.BlockSpec((own, cols), lambda i, m: (0, 0)), pl.BlockSpec((n_cb, own, 128), lambda i, m: (0, 0, 0))]),
         out_shape=[jax.ShapeDtypeStruct((own, cols), F32), jax.ShapeDtypeStruct((n_cb, own, 128), F32)], name="fold", compiler_params=SMALL)(

time: 92.1 us -> 92.1 us (level)
  no operation moved by 1% of the time
where the time goes in v7:
time: 92.1 us; the launch traced here: 91.7 us
  blocking collectives  70.2 us (76%)
  starting transfers between devices  12.8 us (14%)
  waiting for transfers between devices  5 us (5%)
  Pallas kernels  3.72 us (4%)
    all_to_all x3, blocking collectives, exchange(): return lax.all_to_all(array, axes, split_axis=0, concat_axis=0, tiled=True)  70.2 us
    ppermute x3, starting transfers between devices, body(): others.append(lax.ppermute(mine, QUAD, [(i, i ^ k) for i in range(n_quad)]))  8.37 us
    ppermute x3, waiting for transfers between devices, body(): others.append(lax.ppermute(mine, QUAD, [(i, i ^ k) for i in range(n_quad)]))  5 us
    all_to_all x1, starting transfers between devices, exchange(): return lax.all_to_all(array, axes, split_axis=0, concat_axis=0, tiled=True)  4.41 us
  transfers between devices with their start and end apart: 4, of which 3 were waited for; matrix products, arithmetic and copies ran while one was open for 0% of the time, Pallas kernels for 0%

profile of v7, /device:TPU:1, one launch (start us, length us, event | category | flops | bytes accessed | tf_op | source)
XLA Modules:
  0.0 91.7 jit_solution(14309122474588496108)
XLA Ops:
  0.0 1.7 %enter.1 = (f32[88,512]{1,0:T(8,128)S(1)}, bf16[512]{0:T(512)(128)(2,1)S(1)}, bf16[8,512]{1,0:T(8,128)(2,1)S(1)}, f32[8,96,128]{2,1,0:T(8,128)S(1)}) custom-call(s32[1]{0:T(128)} %bitcast.here, bf16[88,512]{1,0:T(8,128)(2,1)} %down_hbm.1, bf16[512,512]{1,0:T(8,128)(2,1)} %tok_hbm.1, bf16[512]{0:T(512)(128)(2,1)} %gain_hbm.1, bf16[88,512]{1,0:T(8,128)(2,1)} %bitcast.6, ...), custom_call_target="tpu_custom_call" | custom-call | tf_op jit(solution)/shard_map/enter/pallas_call | solution.py:144
  1.7 24.5 %all_to_all.20.parts = f32[8,96,128]{2,1,0:T(8,128)S(1)} all-to-all(f32[8,96,128]{2,1,0:T(8,128)S(1)} %get-tuple-element.11), channel_id=1, replica_groups=mesh['zq'=8,'z0'=2,'yq'=4,'y0'=2,'cb'=8] {'cb'}, dimensions={0} | all-to-all | bytes 786432 | tf_op jit(solution)/shard_map/all_to_all | solution.py:22
  26.3 0.9 middle.1
  27.2 4.4 %all-to-all-start.1 = ((f32[32,16,88]{2,1,0:T(8,128)}), f32[32,16,88]{2,1,0:T(8,128)S(1)}, u32[]{:S(2)}, u32[]{:S(2)}) async-start(f32[32,16,88]{2,1,0:T(8,128)} %bitcast.3), calls=%async_computation.1 | async-start | bytes 524288 | tf_op jit(solution)/shard_map/all_to_all | solution.py:22
  31.6 4.2 %collective-permute-start.2 = (f32[88,512]{1,0:T(8,128)S(1)}, f32[88,512]{1,0:T(8,128)S(1)}, u32[]{:S(2)}, u32[]{:S(2)}) collective-permute-start(f32[88,512]{1,0:T(8,128)S(1)} %get-tuple-element.12.w0), channel_id=1, source_target_pairs={{0,72},{8,64},{64,8},{72,0},{1,73},{9,65},{65,9},{73,1},{2,74},{10... | collective-permute-start | bytes 540680 | tf_op jit(solution)/shard_map/ppermute | solution.py:156
  35.8 2.2 %collective-permute-start.1 = (f32[88,512]{1,0:T(8,128)S(1)}, f32[88,512]{1,0:T(8,128)S(1)}, u32[]{:S(2)}, u32[]{:S(2)}) collective-permute-start(f32[88,512]{1,0:T(8,128)S(1)} %get-tuple-element.12.w0), channel_id=1, source_target_pairs={{0,64},{8,72},{64,0},{72,8},{1,65},{9,73},{65,1},{73,9},{2,66},{10... | collective-permute-start | bytes 540680 | tf_op jit(solution)/shard_map/ppermute | solution.py:156
  37.9 2.0 %collective-permute-start = (f32[88,512]{1,0:T(8,128)S(1)}, f32[88,512]{1,0:T(8,128)S(1)}, u32[]{:S(2)}, u32[]{:S(2)}) collective-permute-start(f32[88,512]{1,0:T(8,128)S(1)} %get-tuple-element.12.w0), channel_id=1, source_target_pairs={{0,8},{8,0},{64,72},{72,64},{1,9},{9,1},{65,73},{73,65},{2,10},{10... | collective-permute-start | bytes 540680 | tf_op jit(solution)/shard_map/ppermute | solution.py:156
  40.0 0.0 all-to-all-done.1
  40.0 1.3 %collective-permute-done.2.w3 = f32[88,512]{1,0:T(8,128)S(1)} collective-permute-done((f32[88,512]{1,0:T(8,128)S(1)}, f32[88,512]{1,0:T(8,128)S(1)}, u32[]{:S(2)}, u32[]{:S(2)}) %collective-permute-start.2) | collective-permute-done | bytes 180256 | tf_op jit(solution)/shard_map/ppermute | solution.py:156
  41.3 2.9 %collective-permute-done.1.w2 = f32[88,512]{1,0:T(8,128)S(1)} collective-permute-done((f32[88,512]{1,0:T(8,128)S(1)}, f32[88,512]{1,0:T(8,128)S(1)}, u32[]{:S(2)}, u32[]{:S(2)}) %collective-permute-start.1) | collective-permute-done | bytes 180256 | tf_op jit(solution)/shard_map/ppermute | solution.py:156
  44.2 0.8 collective-permute-done.w1
  45.0 0.3 back.1
  45.3 31.6 %all_to_all.21.sums = f32[32,16,128]{2,1,0:T(8,128)S(1)} all-to-all(f32[32,16,128]{2,1,0:T(8,128)S(1)} %back.1), channel_id=1, replica_groups=mesh['zq'=8,'z0'=2,'yq'=4,'y0'=2,'cb'=8] {'zq','yq'}, dimensions={0} | all-to-all | bytes 524288 | tf_op jit(solution)/shard_map/all_to_all | solution.py:22
  76.9 0.1 fold.1
  77.0 14.0 %all_to_all.22.sq = f32[8,4,128]{2,1,0:T(4,128)S(1)} all-to-all(f32[8,4,128]{2,1,0:T(4,128)S(1)} %get-tuple-element.16), channel_id=1, replica_groups=mesh['zq'=8,'z0'=2,'yq'=4,'y0'=2,'cb'=8] {'cb'}, dimensions={0} | all-to-all | bytes 32768 | tf_op jit(solution)/shard_map/all_to_all | solution.py:22
  91.0 0.7 finish.1
  (1 shorter events, 0.0 us)
Async XLA Ops:
  27.2 12.8 %all-to-all-start.1 = ((f32[32,16,88]{2,1,0:T(8,128)}), f32[32,16,88]{2,1,0:T(8,128)S(1)}, u32[]{:S(2)}, u32[]{:S(2)}) async-start(f32[32,16,88]{2,1,0:T(8,128)} %bitcast.3), calls=%async_computation.1 | async-start | bytes 524288 | tf_op jit(solution)/shard_map/all_to_all | solution.py:22
  31.6 9.7 %collective-permute-start.2 = (f32[88,512]{1,0:T(8,128)S(1)}, f32[88,512]{1,0:T(8,128)S(1)}, u32[]{:S(2)}, u32[]{:S(2)}) collective-permute-start(f32[88,512]{1,0:T(8,128)S(1)} %get-tuple-element.12.w0), channel_id=1, source_target_pairs={{0,72},{8,64},{64,8},{72,0},{1,73},{9,65},{65,9},{73,1},{2,74},{10... | collective-permute-start | bytes 540680 | tf_op jit(solution)/shard_map/ppermute | solution.py:156
  35.8 8.5 %collective-permute-start.1 = (f32[88,512]{1,0:T(8,128)S(1)}, f32[88,512]{1,0:T(8,128)S(1)}, u32[]{:S(2)}, u32[]{:S(2)}) collective-permute-start(f32[88,512]{1,0:T(8,128)S(1)} %get-tuple-element.12.w0), channel_id=1, source_target_pairs={{0,64},{8,72},{64,0},{72,8},{1,65},{9,73},{65,1},{73,9},{2,66},{10... | collective-permute-start | bytes 540680 | tf_op jit(solution)/shard_map/ppermute | solution.py:156
  37.9 7.1 %collective-permute-start = (f32[88,512]{1,0:T(8,128)S(1)}, f32[88,512]{1,0:T(8,128)S(1)}, u32[]{:S(2)}, u32[]{:S(2)}) collective-permute-start(f32[88,512]{1,0:T(8,128)S(1)} %get-tuple-element.12.w0), channel_id=1, source_target_pairs={{0,8},{8,0},{64,72},{72,64},{1,9},{9,1},{65,73},{73,65},{2,10},{10... | collective-permute-start | bytes 540680 | tf_op jit(solution)/shard_map/ppermute | solution.py:156

commit v8 on v7

--- a/solution.py
+++ b/solution.py
@@ -22,18 +22,30 @@
     return lax.all_to_all(array, axes, split_axis=0, concat_axis=0, tiled=True)
 
 
-def enter(here, down_hbm, tok_hbm, gain_hbm, wg_hbm, wu_hbm, last_hbm, wide, last, own, out, narrow, tok, gain, wg, wu, sems):
+def enter(here, down_hbm, tok_hbm, gain_hbm, wg_hbm, wu_hbm, last_hbm, wide, last, own, out, narrow, tok, gain, wg, wu, ready, sems):
     rows = own.shape[0]
     source = tok_hbm.at[pl.ds(pl.multiple_of(here[0] // 2 * rows, rows), rows)]
-    pairs = ((down_hbm, narrow), (wg_hbm, wg), (wu_hbm, wu), (gain_hbm, gain), (tok_hbm, tok), (last_hbm, last), (source, own))
+    halves = 2
+    tokens = tok.shape[0] // halves
+    cuts = [pl.ds(h * tokens, tokens) for h in range(halves)]
+    pairs = ((down_hbm, narrow), (wg_hbm, wg), (wu_hbm, wu), (gain_hbm, gain), *[(tok_hbm.at[c], tok.at[c]) for c in cuts],
+             (last_hbm, last), (source, own))
     pending = [pltpu.make_async_copy(a, b, sems.at[k]) for k, (a, b) in enumerate(pairs)]
     for c in pending:
         c.start()
     pending[0].wait()
     wide[...] = narrow[...].astype(F32)
-    for c in pending[1:]:
+    for c in pending[1:4]:
         c.wait()
-    front(tok, gain, wg, wu, out)
+    peers = ready.shape[0] // halves
+    sent = []
+    for h in range(halves):
+        pending[4 + h].wait()
+        front(tok.at[cuts[h]], gain, wg, wu, ready.at[pl.ds(h * peers, peers)])
+        sent.append(pltpu.make_async_copy(ready.at[pl.ds(h * peers, peers)], out.at[pl.ds(h * peers, peers)], sems.at[len(pairs) + h]))
+        sent[h].start()
+    for c in pending[4 + halves :] + sent:
+        c.wait()
 
 
 def order(here, hid, out):
@@ -145,9 +157,10 @@
         enter,
         grid_spec=pltpu.PrefetchScalarGridSpec(
             num_scalar_prefetch=1, grid=(1,), in_specs=[pl.BlockSpec(memory_space=pltpu.HBM)] * 6,
-            out_specs=[whole(units, cols), whole(cols), whole(2 * own, cols), whole(n_cb, packed, lanes)],
+            out_specs=[whole(units, cols), whole(cols), whole(2 * own, cols), pl.BlockSpec(memory_space=pltpu.HBM)],
             scratch_shapes=[pltpu.VMEM((units, cols), BF16), pltpu.VMEM((rows, cols), BF16), pltpu.VMEM((cols,), BF16),
-                            pltpu.VMEM((units, cols), BF16), pltpu.VMEM((units, cols), BF16), pltpu.SemaphoreType.DMA((7,))]),
+                            pltpu.VMEM((units, cols), BF16), pltpu.VMEM((units, cols), BF16), pltpu.VMEM((n_cb, packed, lanes), F32),
+                            pltpu.SemaphoreType.DMA((10,))]),
         out_shape=[jax.ShapeDtypeStruct((units, cols), F32), jax.ShapeDtypeStruct((cols,), BF16), jax.ShapeDtypeStruct((2 * own, cols), BF16),
                    jax.ShapeDtypeStruct((n_cb, packed, lanes), F32)],
         name="enter", compiler_params=SMALL)(here, *hbm)

time: 92.1 us -> 92.7 us (level)
  no operation moved by 1% of the time
where the time goes in v8:
time: 92.7 us; the launch traced here: 92.3 us
  blocking collectives  70.2 us (76%)
  starting transfers between devices  12.8 us (14%)
  waiting for transfers between devices  5 us (5%)
  Pallas kernels  4.31 us (5%)
    all_to_all x3, blocking collectives, exchange(): return lax.all_to_all(array, axes, split_axis=0, concat_axis=0, tiled=True)  70.2 us
    ppermute x3, starting transfers between devices, body(): others.append(lax.ppermute(mine, QUAD, [(i, i ^ k) for i in range(n_quad)]))  8.37 us
    ppermute x3, waiting for transfers between devices, body(): others.append(lax.ppermute(mine, QUAD, [(i, i ^ k) for i in range(n_quad)]))  5 us
    all_to_all x1, starting transfers between devices, exchange(): return lax.all_to_all(array, axes, split_axis=0, concat_axis=0, tiled=True)  4.41 us
    pallas_call x1, Pallas kernels, body(): pl.pallas_call(enter, grid_spec=pltpu.PrefetchScalarGridSpec(num_scalar_p...  2.3 us
  transfers between devices with their start and end apart: 4, of which 3 were waited for; matrix products, arithmetic and copies ran while one was open for 0% of the time, Pallas kernels for 0%

profile of v8, /device:TPU:1, one launch (start us, length us, event | category | flops | bytes accessed | tf_op | source)
XLA Modules:
  0.0 92.3 jit_solution(13023418295861732852)
XLA Ops:
  0.0 2.3 %enter.1 = (f32[88,512]{1,0:T(8,128)S(1)}, bf16[512]{0:T(512)(128)(2,1)S(1)}, bf16[8,512]{1,0:T(8,128)(2,1)S(1)}, f32[8,96,128]{2,1,0:T(8,128)S(1)}) custom-call(s32[1]{0:T(128)} %bitcast.here, bf16[88,512]{1,0:T(8,128)(2,1)} %down_hbm.1, bf16[512,512]{1,0:T(8,128)(2,1)} %tok_hbm.1, bf16[512]{0:T(512)(128)(2,1)} %gain_hbm.1, bf16[88,512]{1,0:T(8,128)(2,1)} %bitcast.6, ...), custom_call_target="tpu_custom_call" | custom-call | tf_op jit(solution)/shard_map/enter/pallas_call | solution.py:156
  2.3 24.5 %all_to_all.20.parts = f32[8,96,128]{2,1,0:T(8,128)S(1)} all-to-all(f32[8,96,128]{2,1,0:T(8,128)S(1)} %get-tuple-element.11), channel_id=1, replica_groups=mesh['zq'=8,'z0'=2,'yq'=4,'y0'=2,'cb'=8] {'cb'}, dimensions={0} | all-to-all | bytes 786432 | tf_op jit(solution)/shard_map/all_to_all | solution.py:22
  26.9 0.9 middle.1
  27.7 4.4 %all-to-all-start.1 = ((f32[32,16,88]{2,1,0:T(8,128)}), f32[32,16,88]{2,1,0:T(8,128)S(1)}, u32[]{:S(2)}, u32[]{:S(2)}) async-start(f32[32,16,88]{2,1,0:T(8,128)} %bitcast.3), calls=%async_computation.1 | async-start | bytes 524288 | tf_op jit(solution)/shard_map/all_to_all | solution.py:22
  32.2 4.2 %collective-permute-start.2 = (f32[88,512]{1,0:T(8,128)S(1)}, f32[88,512]{1,0:T(8,128)S(1)}, u32[]{:S(2)}, u32[]{:S(2)}) collective-permute-start(f32[88,512]{1,0:T(8,128)S(1)} %get-tuple-element.12.w0), channel_id=1, source_target_pairs={{0,72},{8,64},{64,8},{72,0},{1,73},{9,65},{65,9},{73,1},{2,74},{10... | collective-permute-start | bytes 540680 | tf_op jit(solution)/shard_map/ppermute | solution.py:169
  36.3 2.2 %collective-permute-start.1 = (f32[88,512]{1,0:T(8,128)S(1)}, f32[88,512]{1,0:T(8,128)S(1)}, u32[]{:S(2)}, u32[]{:S(2)}) collective-permute-start(f32[88,512]{1,0:T(8,128)S(1)} %get-tuple-element.12.w0), channel_id=1, source_target_pairs={{0,64},{8,72},{64,0},{72,8},{1,65},{9,73},{65,1},{73,9},{2,66},{10... | collective-permute-start | bytes 540680 | tf_op jit(solution)/shard_map/ppermute | solution.py:169
  38.5 2.0 %collective-permute-start = (f32[88,512]{1,0:T(8,128)S(1)}, f32[88,512]{1,0:T(8,128)S(1)}, u32[]{:S(2)}, u32[]{:S(2)}) collective-permute-start(f32[88,512]{1,0:T(8,128)S(1)} %get-tuple-element.12.w0), channel_id=1, source_target_pairs={{0,8},{8,0},{64,72},{72,64},{1,9},{9,1},{65,73},{73,65},{2,10},{10... | collective-permute-start | bytes 540680 | tf_op jit(solution)/shard_map/ppermute | solution.py:169
  40.6 0.0 all-to-all-done.1
  40.6 1.3 %collective-permute-done.2.w3 = f32[88,512]{1,0:T(8,128)S(1)} collective-permute-done((f32[88,512]{1,0:T(8,128)S(1)}, f32[88,512]{1,0:T(8,128)S(1)}, u32[]{:S(2)}, u32[]{:S(2)}) %collective-permute-start.2) | collective-permute-done | bytes 180256 | tf_op jit(solution)/shard_map/ppermute | solution.py:169
  41.9 2.9 %collective-permute-done.1.w2 = f32[88,512]{1,0:T(8,128)S(1)} collective-permute-done((f32[88,512]{1,0:T(8,128)S(1)}, f32[88,512]{1,0:T(8,128)S(1)}, u32[]{:S(2)}, u32[]{:S(2)}) %collective-permute-start.1) | collective-permute-done | bytes 180256 | tf_op jit(solution)/shard_map/ppermute | solution.py:169
  44.8 0.8 collective-permute-done.w1
  45.6 0.3 back.1
  45.9 31.6 %all_to_all.21.sums = f32[32,16,128]{2,1,0:T(8,128)S(1)} all-to-all(f32[32,16,128]{2,1,0:T(8,128)S(1)} %back.1), channel_id=1, replica_groups=mesh['zq'=8,'z0'=2,'yq'=4,'y0'=2,'cb'=8] {'zq','yq'}, dimensions={0} | all-to-all | bytes 524288 | tf_op jit(solution)/shard_map/all_to_all | solution.py:22
  77.5 0.1 fold.1
  77.6 14.0 %all_to_all.22.sq = f32[8,4,128]{2,1,0:T(4,128)S(1)} all-to-all(f32[8,4,128]{2,1,0:T(4,128)S(1)} %get-tuple-element.16), channel_id=1, replica_groups=mesh['zq'=8,'z0'=2,'yq'=4,'y0'=2,'cb'=8] {'cb'}, dimensions={0} | all-to-all | bytes 32768 | tf_op jit(solution)/shard_map/all_to_all | solution.py:22
  91.6 0.7 finish.1
  (1 shorter events, 0.0 us)
Async XLA Ops:
  27.7 12.8 %all-to-all-start.1 = ((f32[32,16,88]{2,1,0:T(8,128)}), f32[32,16,88]{2,1,0:T(8,128)S(1)}, u32[]{:S(2)}, u32[]{:S(2)}) async-start(f32[32,16,88]{2,1,0:T(8,128)} %bitcast.3), calls=%async_computation.1 | async-start | bytes 524288 | tf_op jit(solution)/shard_map/all_to_all | solution.py:22
  32.2 9.7 %collective-permute-start.2 = (f32[88,512]{1,0:T(8,128)S(1)}, f32[88,512]{1,0:T(8,128)S(1)}, u32[]{:S(2)}, u32[]{:S(2)}) collective-permute-start(f32[88,512]{1,0:T(8,128)S(1)} %get-tuple-element.12.w0), channel_id=1, source_target_pairs={{0,72},{8,64},{64,8},{72,0},{1,73},{9,65},{65,9},{73,1},{2,74},{10... | collective-permute-start | bytes 540680 | tf_op jit(solution)/shard_map/ppermute | solution.py:169
  36.3 8.5 %collective-permute-start.1 = (f32[88,512]{1,0:T(8,128)S(1)}, f32[88,512]{1,0:T(8,128)S(1)}, u32[]{:S(2)}, u32[]{:S(2)}) collective-permute-start(f32[88,512]{1,0:T(8,128)S(1)} %get-tuple-element.12.w0), channel_id=1, source_target_pairs={{0,64},{8,72},{64,0},{72,8},{1,65},{9,73},{65,1},{73,9},{2,66},{10... | collective-permute-start | bytes 540680 | tf_op jit(solution)/shard_map/ppermute | solution.py:169
  38.5 7.1 %collective-permute-start = (f32[88,512]{1,0:T(8,128)S(1)}, f32[88,512]{1,0:T(8,128)S(1)}, u32[]{:S(2)}, u32[]{:S(2)}) collective-permute-start(f32[88,512]{1,0:T(8,128)S(1)} %get-tuple-element.12.w0), channel_id=1, source_target_pairs={{0,8},{8,0},{64,72},{72,64},{1,9},{9,1},{65,73},{73,65},{2,10},{10... | collective-permute-start | bytes 540680 | tf_op jit(solution)/shard_map/ppermute | solution.py:169
